TPU v7x, 256 devices: a 4x2x16 block of a 4x16x16 slice. The times are simulated.
256 devices in a mesh: grp: 2 (over y), sp: 16 (over z), tp: 4 (over x), dp: 2 (over core).
Axes of the slice: x: 4, y: 2, z: 16, core: 2. Of those that a mesh axis runs over, the one named last changes fastest.
The devices are a block of a 4x16x16 slice.
Arguments:
- latent: bfloat16 [24576, 4096], P(('grp', 'sp', 'dp')), parts along dimension 0, may hold values from -6 to 6
- context: bfloat16 [1024, 4096], P(('grp', 'sp')), parts along dimension 0, may hold values from -6 to 6
- condition: bfloat16 [8192], P('grp'), parts along dimension 0, may hold values from -6 to 6
- context_condition: bfloat16 [4096], replicated, may hold values from -6 to 6
- shift_weight: bfloat16 [4096, 4096], P('sp', ('tp', 'dp')), may hold values from -0.09375 to 0.09375
- scale_weight: bfloat16 [4096, 4096], P('sp', ('tp', 'dp')), may hold values from -0.09375 to 0.09375
- gate_weight: bfloat16 [4096, 4096], P('sp', ('tp', 'dp')), may hold values from -0.09375 to 0.09375
- norm_gain: float32 [4096], replicated, may hold values from 0.1 to 1.9
- out_gate_weight: bfloat16 [4096, 2048], P(None, ('tp', 'dp')), may hold values from -0.09375 to 0.09375
- signal_weight: bfloat16 [4096, 2048], P(None, ('tp', 'dp')), may hold values from -0.09375 to 0.09375
- writer_weight: bfloat16 [4096, 1024], P(None, ('tp', 'dp')), may hold values from -0.09375 to 0.09375
- reader_matrix: bfloat16 [4096, 1024], P(None, ('tp', 'dp')), may hold values from -0.09375 to 0.09375
- step_weight: bfloat16 [2, 4096, 32], P(None, None, ('tp', 'dp')), may hold values from -0.09375 to 0.09375
- signal_taps: float32 [3, 2048], P(None, ('tp', 'dp')), may hold values from -3.5 to 3.5
- writer_taps: float32 [3, 1024], P(None, ('tp', 'dp')), may hold values from -3.5 to 3.5
- reader_taps: float32 [3, 1024], P(None, ('tp', 'dp')), may hold values from -3.5 to 3.5
- step_bias: float32 [2, 32], P(None, ('tp', 'dp')), may hold values from -4.5 to -2.5
- decay_log: float32 [2, 32], P(None, ('tp', 'dp')), may hold values from -12 to 1
- decay_extra: float32 [2, 32, 24576], P(None, ('tp', 'dp'), ('grp', 'sp')), parts along dimension 2, may hold values from -3 to 0
- group_gain: float32 [2048], P(('tp', 'dp')), may hold values from 0.1 to 1.9
- output_weight: bfloat16 [2048, 4096], P(None, ('tp', 'dp')), may hold values from -0.125 to 0.125
Outputs:
- updated: bfloat16 [24576, 4096], P(('grp', 'sp'), ('tp', 'dp')), parts along dimension 0
There are 2 independent parts, one for each index of `grp`. A program takes and returns all parts, laid end to end along the dimension named above; an argument that names none is the same for every part. Nothing has to cross between parts.
All inputs are finite; a program needn't handle non-finite values.
Results may differ from a plain program's by a relative error of at most 0.007.
Values may be sent and summed in bfloat16 or wider, within the bound.
A program may use at most 128 MiB of HBM per device.

v0:
```python
import jax
import jax.numpy as jnp
from jax import lax
from jax.sharding import PartitionSpec as P

STATE = 128
BLOCK = 128


EPSILON = 1e-06


def copy_for_each(x, axis):
    copies = jnp.broadcast_to(x, (lax.axis_size(axis), *x.shape))
    return lax.all_to_all(copies, axis, split_axis=0, concat_axis=0, tiled=True)


def of_everyone(x, axis):
    everything = copy_for_each(x, axis)
    return jnp.sum(everything, axis=0)


def in_one(arrays, axis):
    ends = [0]
    for a in arrays:
        ends.append(ends[-1] + a.size)
    subtotal = of_everyone(jnp.concatenate([a.ravel() for a in arrays]), axis)
    return tuple((subtotal[b:e].reshape(a.shape) for a, b, e in zip(arrays, ends, ends[1:])))


def side_by_side(arrays, axis, dim, along):
    ends, at = ([], 0)
    for a in arrays[:-1]:
        at += a.shape[along]
        ends.append(at)
    both = jnp.concatenate(arrays, axis=along)
    return tuple(jnp.split(lax.all_gather(both, axis, axis=dim, tiled=True), ends, axis=along))


def rows_first(arrays, axis, dims):
    turned = [jnp.moveaxis(a, dim, 0) for a, dim in zip(arrays, dims)]
    widths = [t[0].size for t in turned]
    both = jnp.concatenate([t.reshape(-1, w) for t, w in zip(turned, widths)], axis=1)
    out = lax.all_gather(both, axis, axis=0, tiled=True)
    tiles = jnp.split(out, [sum(widths[:k]) for k in range(1, len(widths))], axis=1)
    return tuple(
        (
            jnp.moveaxis(b.reshape(-1, *t.shape[1:]), 0, dim)
            for b, t, dim in zip(tiles, turned, dims)
        )
    )


def extended(cells, sides, width):
    for axis, dim in sides:
        count = lax.axis_size(axis)
        ends = count - 1
        head = lax.slice_in_dim(cells, 0, width, axis=dim)
        tail = lax.slice_in_dim(cells, cells.shape[dim] - width, cells.shape[dim], axis=dim)
        cells = jnp.concatenate(
            [
                lax.ppermute(tail, axis, [(i, (i + 1) % count) for i in range(ends)]),
                cells,
                lax.ppermute(head, axis, [((i + 1) % count, i) for i in range(ends)]),
            ],
            axis=dim,
        )
    return cells


def entering(x, axis, combine, identity, reverse):
    devices, position = (lax.axis_size(axis), lax.axis_index(axis))
    everything = jax.tree.map(lambda part: lax.all_gather(part, axis), x)
    start = jax.tree.map(
        lambda part, zero: jnp.broadcast_to(jnp.asarray(zero, part.dtype), part.shape), x, identity
    )

    def turn(k, before):
        at = devices - 1 - k if reverse else k
        reached = at > position if reverse else at < position
        new = combine(before, jax.tree.map(lambda part: part[at], everything))
        return jax.tree.map(lambda a, b: jnp.where(reached, a, b), new, before)

    return lax.fori_loop(0, devices, turn, start)


def modulate(rows, norm_gain, shift_vec, scale_vec):
    values = rows.astype(jnp.float32)
    normed = (
        values * lax.rsqrt(jnp.mean(values * values, axis=-1, keepdims=True) + EPSILON) * norm_gain
    )
    return (normed * (1.0 + scale_vec) + shift_vec).astype(jnp.bfloat16)


def centred_conv(padded, conv_taps, length):
    running = jnp.zeros((length, padded.shape[1]), jnp.float32)
    for offset in range(conv_taps.shape[0]):
        running = running + conv_taps[offset] * padded[offset : offset + length].astype(jnp.float32)
    return jax.nn.silu(running)


def project_rows(hidden, signal_weight, writer_weight, reader_matrix, step_weight):
    raw_cols = jnp.concatenate(
        [
            jnp.dot(hidden, signal_weight, preferred_element_type=jnp.float32),
            jnp.dot(hidden, writer_weight, preferred_element_type=jnp.float32),
            jnp.dot(hidden, reader_matrix, preferred_element_type=jnp.float32),
        ],
        axis=1,
    ).astype(jnp.bfloat16)
    step_in = jnp.stack(
        [
            jnp.dot(hidden, step_weight[0], preferred_element_type=jnp.float32),
            jnp.dot(hidden, step_weight[1], preferred_element_type=jnp.float32),
        ]
    ).astype(jnp.bfloat16)
    return (raw_cols, step_in)


def split_mixed(conv_out, head_count, head_width, group_count, state_width):
    length = conv_out.shape[0]
    signal_end = head_count * head_width
    writer_end = signal_end + group_count * state_width
    signal = conv_out[:, :signal_end].reshape(length, head_count, head_width)
    writer = conv_out[:, signal_end:writer_end].reshape(length, group_count, state_width)
    reader = conv_out[:, writer_end:].reshape(length, group_count, state_width)
    return (signal, writer, reader)


def state_span(signal, step_size, log_decay, writer, reader, start_state, block):
    length, head_count, head_width = signal.shape
    group_count, state_width = (writer.shape[1], writer.shape[2])
    per_group = head_count // group_count
    blocks = length // block
    scaled = (signal * step_size[..., None]).reshape(
        blocks, block, group_count, per_group, head_width
    )
    cum_log = jnp.cumsum(log_decay.reshape(blocks, block, group_count, per_group), axis=1)
    writer_blk = writer.reshape(blocks, block, group_count, state_width)
    reader_blk = reader.reshape(blocks, block, group_count, state_width)
    inner_dot = jnp.einsum("bign,bjgn->bgij", reader_blk, writer_blk)
    moved = jnp.moveaxis(cum_log, 1, -1)
    gap_logs = moved[..., :, None] - moved[..., None, :]
    lower_mask = jnp.tril(jnp.ones((block, block), dtype=bool))
    weights = jnp.exp(jnp.where(lower_mask, gap_logs, -jnp.inf))
    in_block = jnp.einsum("bgij,bgeij,bjgep->bigep", inner_dot, weights, scaled)
    to_end = jnp.exp(cum_log[:, -1:] - cum_log)
    states = jnp.einsum("bjgn,bjge,bjgep->bgepn", writer_blk, to_end, scaled)
    block_decay = jnp.exp(cum_log[:, -1])

    def advance(running, block_item):
        state_add, decay_now = block_item
        return (running * decay_now[..., None, None] + state_add, running)

    last_state, before = lax.scan(
        advance,
        start_state.reshape(group_count, per_group, head_width, state_width),
        (states, block_decay),
    )
    carried = jnp.einsum("bign,bgepn,bige->bigep", reader_blk, before, jnp.exp(cum_log))
    result = (in_block + carried).reshape(length, head_count, head_width)
    return (result, last_state.reshape(head_count, head_width, state_width))


def context_state(signal, row_weights, writer):
    length, head_count, head_width = signal.shape
    group_count, state_width = (writer.shape[1], writer.shape[2])
    per_group = head_count // group_count
    grouped = signal.reshape(length, group_count, per_group, head_width)
    weights = row_weights.reshape(length, group_count, per_group)
    summed = jnp.einsum("tgn,tge,tgep->gepn", writer, weights, grouped)
    return summed.reshape(head_count, head_width, state_width)


def group_norm(gated, group_count, group_gain):
    length = gated.shape[0]
    grouped = gated.reshape(length, group_count, -1)
    normed = grouped * lax.rsqrt(jnp.mean(grouped * grouped, axis=-1, keepdims=True) + EPSILON)
    return (normed.reshape(length, -1) * group_gain).astype(jnp.bfloat16)


def chain_step(preceding_entries, later):
    return (
        preceding_entries[0] + later[0],
        jnp.exp(later[0])[:, None, None] * preceding_entries[1] + later[1],
    )


def on_device(
    latent,
    context,
    condition,
    context_condition,
    shift_weight,
    scale_weight,
    gate_weight,
    norm_gain,
    out_gate_weight,
    signal_weight,
    writer_weight,
    reader_matrix,
    step_weight,
    signal_taps,
    writer_taps,
    reader_taps,
    step_bias,
    decay_log,
    decay_extra,
    group_gain,
    output_weight,
):
    rows_here = shift_weight.shape[0]
    cond_act = jax.nn.silu(jnp.stack([condition, context_condition]).astype(jnp.float32)).astype(
        jnp.bfloat16
    )
    own_rows = lax.dynamic_slice_in_dim(cond_act, lax.axis_index("sp") * rows_here, rows_here, 1)
    shift_part = jnp.dot(own_rows, shift_weight, preferred_element_type=jnp.float32)
    scale_part = jnp.dot(own_rows, scale_weight, preferred_element_type=jnp.float32)
    gate_part = jnp.dot(own_rows[:1], gate_weight, preferred_element_type=jnp.float32)
    shift_sum, scale_sum, gate_sum = in_one((shift_part, scale_part, gate_part), "sp")
    shift_vec, scale_vec = side_by_side((shift_sum, scale_sum), ("tp", "dp"), 1, 0)
    gate_vec = gate_sum[0]
    full_rows = lax.all_gather(latent, "dp", axis=0, tiled=True)
    length = full_rows.shape[0]
    hidden = modulate(full_rows, norm_gain, shift_vec[0], scale_vec[0])
    ctx_hidden = modulate(context, norm_gain, shift_vec[1], scale_vec[1])
    conv_taps = jnp.concatenate([signal_taps, writer_taps, reader_taps], axis=1)
    decay_rates = -jnp.exp(decay_log)[:, None, :]
    head_count = step_bias.shape[1]
    head_width = signal_weight.shape[1] // head_count
    group_count = writer_weight.shape[1] // STATE
    per_group = head_count // group_count
    ctx_raw, ctx_step_in = project_rows(
        ctx_hidden, signal_weight, writer_weight, reader_matrix, step_weight
    )
    every_raw, every_step = rows_first((ctx_raw, ctx_step_in), "sp", (0, 1))
    ctx_len = every_raw.shape[0]
    ctx_conv = centred_conv(jnp.pad(every_raw, ((1, 1), (0, 0))), conv_taps, ctx_len)
    ctx_signal, ctx_writer, _ = split_mixed(ctx_conv, head_count, head_width, group_count, STATE)
    prefix_stride_length = jax.nn.softplus(every_step.astype(jnp.float32) + step_bias[:, None, :])
    ctx_decay = decay_rates * prefix_stride_length
    cum_log = jnp.cumsum(ctx_decay, axis=1)
    ctx_forward = context_state(
        ctx_signal, jnp.exp(cum_log[0, -1:] - cum_log[0]) * prefix_stride_length[0], ctx_writer
    )
    ctx_backward = context_state(
        ctx_signal, jnp.exp(cum_log[1] - ctx_decay[1]) * prefix_stride_length[1], ctx_writer
    )
    gate_in = jnp.dot(hidden, out_gate_weight, preferred_element_type=jnp.float32).astype(
        jnp.bfloat16
    )
    raw_cols, step_in = project_rows(
        hidden, signal_weight, writer_weight, reader_matrix, step_weight
    )
    padded = extended(raw_cols, (("sp", 0),), 1)
    signal, writer, reader = split_mixed(
        centred_conv(padded, conv_taps, length), head_count, head_width, group_count, STATE
    )
    step_size = jax.nn.softplus(step_in.astype(jnp.float32) + step_bias[:, None, :])
    log_decay = decay_rates * step_size + jnp.swapaxes(decay_extra, 1, 2)
    zero_state = jnp.zeros((head_count, head_width, STATE), jnp.float32)
    forward_out, forward_last = state_span(
        signal, step_size[0], log_decay[0], writer, reader, zero_state, BLOCK
    )
    back_signal = jnp.flip(signal, 0)
    back_reader = jnp.flip(reader, 0)
    back_decay = jnp.flip(log_decay[1], 0)
    backward_out, backward_last = state_span(
        back_signal,
        jnp.flip(step_size[1], 0),
        back_decay,
        jnp.flip(writer, 0),
        back_reader,
        zero_state,
        BLOCK,
    )
    cum_forward = jnp.cumsum(log_decay[0], axis=0)
    cumulative_backward = jnp.cumsum(back_decay, axis=0)
    identity = (jnp.zeros((head_count,), jnp.float32), zero_state)
    onward_inflow = entering((cum_forward[-1], forward_last), "sp", chain_step, identity, False)
    enter_bwd = entering((cumulative_backward[-1], backward_last), "sp", chain_step, identity, True)
    start_fwd = jnp.exp(onward_inflow[0])[:, None, None] * ctx_forward + onward_inflow[1]
    start_bwd = jnp.exp(enter_bwd[0])[:, None, None] * ctx_backward + enter_bwd[1]
    reader_head_rows = jnp.repeat(reader, per_group, axis=1)
    back_heads = jnp.repeat(back_reader, per_group, axis=1)
    forward_out = (
        forward_out
        + jnp.einsum("thn,hpn->thp", reader_head_rows, start_fwd) * jnp.exp(cum_forward)[..., None]
    )
    backward_out = (
        backward_out
        + jnp.einsum("thn,hpn->thp", back_heads, start_bwd)
        * jnp.exp(cumulative_backward)[..., None]
    )
    both = (forward_out + jnp.flip(backward_out, 0)).reshape(length, -1)
    gated = both * jax.nn.silu(gate_in.astype(jnp.float32))
    normed = group_norm(gated, group_count, group_gain)
    mix = jnp.dot(
        lax.all_gather(normed, ("tp", "dp"), axis=1, tiled=True),
        output_weight,
        preferred_element_type=jnp.float32,
    )
    out_start = lax.axis_index(("tp", "dp")) * output_weight.shape[1]
    residual = lax.dynamic_slice_in_dim(full_rows, out_start, output_weight.shape[1], 1).astype(
        jnp.float32
    )
    return (residual + gate_vec * mix).astype(jnp.bfloat16)


def solution(mesh):
    in_specs = (
        P(("grp", "sp", "dp"), None),
        P(("grp", "sp"), None),
        P("grp"),
        P(),
        P("sp", ("tp", "dp")),
        P("sp", ("tp", "dp")),
        P("sp", ("tp", "dp")),
        P(),
        P(None, ("tp", "dp")),
        P(None, ("tp", "dp")),
        P(None, ("tp", "dp")),
        P(None, ("tp", "dp")),
        P(None, None, ("tp", "dp")),
        P(None, ("tp", "dp")),
        P(None, ("tp", "dp")),
        P(None, ("tp", "dp")),
        P(None, ("tp", "dp")),
        P(None, ("tp", "dp")),
        P(None, ("tp", "dp"), ("grp", "sp")),
        P(("tp", "dp")),
        P(None, ("tp", "dp")),
    )
    out_specs = P(("grp", "sp"), ("tp", "dp"))
    return jax.shard_map(
        on_device, mesh=mesh, in_specs=in_specs, out_specs=out_specs, check_vma=False
    )
```

profile of v0, /device:TPU:33, one launch (start us, length us, event | category | flops | bytes accessed | tf_op | source)
XLA Modules:
  0.0 478.3 jit_solution(13487710746028656442)
XLA Ops:
  8.9 24.5 %all-to-all-start = ((f32[16,1,2560]{2,1,0:T(1,128)}), f32[16,1,2560]{2,1,0:T(1,128)S(1)}, u32[]{:S(2)}, u32[]{:S(2)}) async-start(f32[16,1,2560]{2,1,0:T(1,128)} %broadcast_in_dim.34), calls=%async_computation | async-start | bytes 327680 | tf_op jit(solution)/shard_map/all_to_all | solution.py:15
  34.5 10.9 %all-to-all-done = f32[16,1,2560]{2,1,0:T(1,128)S(1)} async-done(((f32[16,1,2560]{2,1,0:T(1,128)}), f32[16,1,2560]{2,1,0:T(1,128)S(1)}, u32[]{:S(2)}, u32[]{:S(2)}) %all-to-all-start) | async-done | bytes 163872 | tf_op jit(solution)/shard_map/all_to_all | solution.py:15
  45.6 17.6 %all_gather.25 = f32[4,4096]{1,0:T(4,128)S(1)} all-gather(f32[4,512]{1,0:T(4,128)S(1)} %pad_maximum_fusion.9), channel_id=1, replica_groups=mesh['grp'=2,'sp'=16,'tp'=4,'dp'=2] {'tp','dp'}, dimensions={1}, use_global_device_ids=true | all-gather | bytes 73728 | tf_op jit(solution)/shard_map/all_gather | solution.py:37
  67.6 25.9 %all_gather.28 = bf16[512,520]{1,0:T(8,128)(2,1)S(1)} all-gather(bf16[32,520]{1,0:T(8,128)(2,1)S(1)} %pad_maximum_fusion.7), channel_id=1, replica_groups=mesh['grp'=2,'sp'=16,'tp'=4,'dp'=2] {'sp'}, dimensions={0}, use_global_device_ids=true | all-gather | bytes 565760 | tf_op jit(solution)/shard_map/all_gather | solution.py:44
  101.1 4.2 fusion.4
  105.7 3.1 fusion.8
  121.2 4.7 collective-permute-start
  128.5 3.3 rev.19
  161.5 20.6 %all-gather.1 = f32[16,1,4]{2,1,0:T(1,128)} all-gather(f32[1,1,4]{2,1,0:T(1,128)} %bitcast.351), channel_id=1, replica_groups=mesh['grp'=2,'sp'=16,'tp'=4,'dp'=2] {'sp'}, dimensions={0}, use_global_device_ids=true | all-gather | bytes 272 | tf_op jit(solution)/shard_map/all_gather | solution.py:73
  182.1 21.8 %all-gather = f32[16,1,4]{2,1,0:T(1,128)} all-gather(f32[1,1,4]{2,1,0:T(1,128)} %bitcast.352), channel_id=1, replica_groups=mesh['grp'=2,'sp'=16,'tp'=4,'dp'=2] {'sp'}, dimensions={0}, use_global_device_ids=true | all-gather | bytes 272 | tf_op jit(solution)/shard_map/all_gather | solution.py:73
  204.0 4.9 %divide_multiply_fusion = f32[768,512]{0,1:T(8,128)S(1)} fusion(bf16[1,512]{0,1:T(8,128)(2,1)S(1)} %collective-permute-done.1, bf16[768,128]{0,1:T(8,128)(2,1)S(1)} %copy-done.15, bf16[768,128]{0,1:T(8,128)(2,1)S(1)} %copy-done.17, bf16[768,256]{0,1:T(8,128)(2,1)} %copy-done.23, bf16[1,512]{0,1:T(8,128)(2,1)} %collective-permute-done, f32[512]{0:T(512)} %bitcast.339, ...), kind=kLoop, calls=%fused_computation.35 | loop fusion | flops 12189696 | bytes 2367488 | tf_op jit(solution)/shard_map/jit(silu)/mul | solution.py:99
  209.8 3.8 reverse.6
  215.3 3.8 reverse.7
  232.5 8.2 %while.62 = (s32[]{:T(128)}, f32[1,4,64,128]{3,2,1,0:T(8,128)S(1)}, bf16[6,1,4,64,128]{4,3,2,1,0:T(8,128)(2,1)}, f32[6,1,4]{2,1,0:T(1,128)}, f32[6,1,4,64,128]{4,3,2,1,0:T(8,128)S(1)}, /*index=5*/s32[]{:T(128)}, s32[]{:T(128)}) while((s32[]{:T(128)}, f32[1,4,64,128]{3,2,1,0:T(8,128)S(1)}, ...), condition=%wide.region_14.15_spmd.clone, body=%wide.region_13.14_spmd.clone.sunk | while | flops 131075 | bytes 589980 | solution.py:155
  253.6 10.1 %while.60 = (s32[]{:T(128)}, f32[1,4,64,128]{3,2,1,0:T(8,128)S(1)}, bf16[6,1,4,64,128]{4,3,2,1,0:T(8,128)(2,1)S(1)}, f32[6,1,4]{2,1,0:T(1,128)}, f32[6,1,4,64,128]{4,3,2,1,0:T(8,128)}, /*index=5*/s32[]{:T(128)}, s32[]{:T(128)}) while((s32[]{:T(128)}, f32[1,4,64,128]{3,2,1,0:T(8,128)S(1)}, ...), condition=%wide.region_4.5_spmd.clone, body=%wide.region_3.4_spmd.clone.sunk | while | flops 131075 | bytes 589980 | solution.py:155
  266.9 52.0 %all-gather.11.cloned.1.call-done = f32[16,4,64,128]{3,2,1,0:T(8,128)} async-done(((f32[1,4,64,128]{3,2,1,0:T(8,128)}), f32[16,4,64,128]{3,2,1,0:T(8,128)}) %all-gather.11.cloned.1.call-update) | async-done | bytes 2097168 | tf_op jit(solution)/shard_map/all_gather | solution.py:73
  318.9 27.4 %while.63 = (s32[]{:T(128)}, f32[4]{0:T(128)S(1)}, f32[4,64,128]{2,1,0:T(8,128)S(1)}, s32[]{:T(128)}, f32[16,4]{1,0:T(8,128)}, /*index=5*/f32[16,4,64,128]{3,2,1...) while((s32[]{:T(128)}, f32[4]{0:T(128)S(1)}, f32[4,64,128]{2,1,0:T(8,128)S(1)}, ...), condition=%wide.region_18.19_spmd.clone, body=%wide.region_17.18_spmd.clone.sunk | while | flops 131092 | bytes 393481 | solution.py:84
  349.1 4.5 rev.20
  353.6 35.5 %all-gather.9.cloned.1.call-done = f32[16,4,64,128]{3,2,1,0:T(8,128)} async-done(((f32[1,4,64,128]{3,2,1,0:T(8,128)}), f32[16,4,64,128]{3,2,1,0:T(8,128)}) %all-gather.9.cloned.1.call-update) | async-done | bytes 2097168 | tf_op jit(solution)/shard_map/all_gather | solution.py:73
  389.1 27.4 %while.61 = (s32[]{:T(128)}, f32[4]{0:T(128)S(1)}, f32[4,64,128]{2,1,0:T(8,128)S(1)}, s32[]{:T(128)}, f32[16,4]{1,0:T(8,128)}, /*index=5*/f32[16,4,64,128]{3,2,1,0:T(8,128)}, s32[]{:T(128)}, s32[]{:T(128)}) while((s32[]{:T(128)}, f32[4]{0:T(128)S(1)}, f32[4,64,128]{2,1,0:T(8,128)S(1)}, s32[]{:T(128)}, f32[16,4]{1,0:T(8,128)}, ...), condition=%wide.region_8.9_spmd.clone, body=%wide.region_7.8_spmd.clone.sunk | while | flops 131088 | bytes 393419 | solution.py:84
  416.5 2.9 fusion.27
  419.4 5.5 %multiply_reduce_fusion = (f32[768]{0:T(1024)S(1)}, f32[768,256]{0,1:T(8,128)S(1)}) fusion(bf16[768,4096]{1,0:T(8,128)(2,1)} %copy-done.1, bf16[4096,256]{1,0:T(8,128)(2,1)} %param.37, f32[768,4,64]{0,2,1:T(8,128)} %fusion.27), kind=kOutput, calls=%fused_computation.95 | convolution fusion | flops 1612381440 | bytes 9964544 | tf_op jit(solution)/shard_map/dot_general | solution.py:249
  425.9 41.1 %all-gather.13.cloned.1.call-done = bf16[768,2048]{0,1:T(8,128)(2,1)} async-done(((bf16[768,256]{0,1:T(8,128)(2,1)}), bf16[768,2048]{0,1:T(8,128)(2,1)}) %all-gather.13.cloned.1.call-update) | async-done | bytes 3145744 | tf_op jit(solution)/shard_map/all_gather | solution.py:299
  467.0 4.8 add_convert_fusion
  (364 shorter events, 167.6 us)
Async XLA Ops:
  6.5 460.5 %copy-start = (bf16[2048,512]{1,0:T(8,128)(2,1)S(1)}, bf16[2048,512]{1,0:T(8,128)(2,1)}, u32[]{:S(2)}) copy-start(bf16[2048,512]{1,0:T(8,128)(2,1)} %param.49) | copy-start | bytes 6291460
  6.6 94.5 %all-gather.7.cloned.1.call-start = ((), (), s32[]{:S(2)}) async-start(), calls=%async_computation.1 | async-start | bytes 9437184 | tf_op jit(solution)/shard_map/all_gather | solution.py:223
  7.4 55.8 %copy-start.31 = (f32[4096]{0:T(1024)S(1)}, f32[4096]{0:T(1024)}, u32[]{:S(2)}) copy-start(f32[4096]{0:T(1024)} %param.36) | copy-start | bytes 49156
  7.4 56.0 %copy-start.28 = (bf16[2,4096,4]{1,2,0:T(4,128)(2,1)S(1)}, bf16[2,4096,4]{1,2,0:T(4,128)(2,1)}, u32[]{:S(2)}) copy-start(bf16[2,4096,4]{1,2,0:T(4,128)(2,1)} %param.41) | copy-start | bytes 196612
  8.9 36.5 %all-to-all-start = ((f32[16,1,2560]{2,1,0:T(1,128)}), f32[16,1,2560]{2,1,0:T(1,128)S(1)}, u32[]{:S(2)}, u32[]{:S(2)}) async-start(f32[16,1,2560]{2,1,0:T(1,128)} %broadcast_in_dim.34), calls=%async_computation | async-start | bytes 327680 | tf_op jit(solution)/shard_map/all_to_all | solution.py:15
  33.4 285.4 %all-gather.11.cloned.1.call-start = ((), (), s32[]{:S(2)}) async-start(), calls=%async_computation.3 | async-start | bytes 2228224 | tf_op jit(solution)/shard_map/all_gather | solution.py:73
  34.4 59.1 %copy-start.41 = (f32[1,512]{1,0:T(1,128)}, f32[1,512]{1,0:T(1,128)S(1)}, u32[]{:S(2)}) copy-start(f32[1,512]{1,0:T(1,128)S(1)} %get-tuple-element.663) | copy-start | bytes 6148
  34.5 59.1 %copy-start.42 = (f32[1,512]{1,0:T(1,128)}, f32[1,512]{1,0:T(1,128)S(1)}, u32[]{:S(2)}) copy-start(f32[1,512]{1,0:T(1,128)S(1)} %get-tuple-element.664) | copy-start | bytes 6148
  34.5 59.1 %copy-start.43 = (f32[1,512]{1,0:T(1,128)}, f32[1,512]{1,0:T(1,128)S(1)}, u32[]{:S(2)}) copy-start(f32[1,512]{1,0:T(1,128)S(1)} %get-tuple-element.665) | copy-start | bytes 6148
  119.9 84.0 %collective-permute-start.1 = (bf16[1,512]{0,1:T(8,128)(2,1)}, bf16[1,512]{0,1:T(8,128)(2,1)S(1)}, u32[]{:S(2)}, u32[]{:S(2)}) collective-permute-start(bf16[1,512]{0,1:T(8,128)(2,1)} %get-tuple-element.645), channel_id=1, source_target_pairs={{8,0},{16,8},{24,16},{32,24},{40,32},{48,40},{56,48},{64,56},{72,6... | collective-permute-start | bytes 3080 | tf_op jit(solution)/shard_map/ppermute | solution.py:64
  121.2 82.7 %collective-permute-start = (bf16[1,512]{0,1:T(8,128)(2,1)}, bf16[1,512]{0,1:T(8,128)(2,1)}, u32[]{:S(2)}, u32[]{:S(2)}) collective-permute-start(bf16[1,512]{0,1:T(8,128)(2,1)} %get-tuple-element.644), channel_id=1, source_target_pairs={{0,8},{8,16},{16,24},{24,32},{32,40},{40,48},{48,56},{56,64},{64,7... | collective-permute-start | bytes 3080 | tf_op jit(solution)/shard_map/ppermute | solution.py:62
  150.0 53.9 %copy-start.15 = (bf16[768,128]{0,1:T(8,128)(2,1)S(1)}, bf16[768,128]{0,1:T(8,128)(2,1)}, u32[]{:S(2)}) copy-start(bf16[768,128]{0,1:T(8,128)(2,1)} %copy-done.14) | copy-start | bytes 589828
  150.0 53.9 %copy-start.17 = (bf16[768,128]{0,1:T(8,128)(2,1)S(1)}, bf16[768,128]{0,1:T(8,128)(2,1)}, u32[]{:S(2)}) copy-start(bf16[768,128]{0,1:T(8,128)(2,1)} %copy-done.16) | copy-start | bytes 589828
  241.5 147.6 %all-gather.9.cloned.1.call-start = ((), (), s32[]{:S(2)}) async-start(), calls=%async_computation.2 | async-start | bytes 2228224 | tf_op jit(solution)/shard_map/all_gather | solution.py:73
  265.2 53.7 %copy-start.46 = (f32[4]{0:T(128)S(1)}, f32[4]{0:T(128)}, u32[]{:S(2)}) copy-start(f32[4]{0:T(128)} %custom-call.4) | copy-start | bytes 52
  266.8 79.6 %copy-start.5 = (f32[512,256]{0,1:T(8,128)S(1)}, f32[512,256]{0,1:T(8,128)}, u32[]{:S(2)}) copy-start(f32[512,256]{0,1:T(8,128)} %copy.318) | copy-start | bytes 1572868
  266.8 79.6 %copy-start.36 = (f32[768,4]{0,1:T(4,128)S(1)}, f32[768,4]{0,1:T(4,128)}, u32[]{:S(2)}) copy-start(f32[768,4]{0,1:T(4,128)} %get-tuple-element.636) | copy-start | bytes 36868
  266.8 79.6 %copy-start.39 = (f32[512,4]{0,1:T(4,128)S(1)}, f32[512,4]{0,1:T(4,128)}, u32[]{:S(2)}) copy-start(f32[512,4]{0,1:T(4,128)} %fusion.94) | copy-start | bytes 24580
  266.8 200.2 %all-gather.13.cloned.1.call-start = ((), (), s32[]{:S(2)}) async-start(), calls=%async_computation.4 | async-start | bytes 3538944 | tf_op jit(solution)/shard_map/all_gather | solution.py:299
  346.4 42.7 %copy-start.45 = (f32[4]{0:T(128)S(1)}, f32[4]{0:T(128)}, u32[]{:S(2)}) copy-start(f32[4]{0:T(128)} %custom-call.1) | copy-start | bytes 52
  349.1 67.4 %copy-start.12 = (bf16[768,128]{1,0:T(8,128)(2,1)S(1)}, bf16[768,128]{1,0:T(8,128)(2,1)}, u32[]{:S(2)}) copy-start(bf16[768,128]{1,0:T(8,128)(2,1)} %copy.303) | copy-start | bytes 589828
  349.1 67.4 %copy-start.35 = (f32[768,4]{0,1:T(4,128)S(1)}, f32[768,4]{0,1:T(4,128)}, u32[]{:S(2)}) copy-start(f32[768,4]{0,1:T(4,128)} %get-tuple-element.632) | copy-start | bytes 36868
  349.1 67.4 %copy-start.38 = (f32[512,4]{0,1:T(4,128)S(1)}, f32[512,4]{0,1:T(4,128)}, u32[]{:S(2)}) copy-start(f32[512,4]{0,1:T(4,128)} %fusion.95) | copy-start | bytes 24580
  424.9 42.1 %slice-start = ((f32[2560]{0:T(1024)}), f32[512]{0:T(512)S(1)}, s32[]{:S(2)}) async-start(f32[2560]{0:T(1024)} %copy-done.37), calls=%async_computation.5 | async-start | bytes 4096 | tf_op jit(solution)/shard_map/slice | solution.py:28
  (40 other events, 267.3 us)
Sparse Core Ops, SparseCore 0:
  9.3 41.3 all-gather.6
  241.6 77.2 all-gather.10
  320.7 68.3 all-gather.8
  426.0 40.9 all-gather.12
where the time goes:
time: 482 us; the launch traced here: 478 us
  waiting for transfers between devices  140 us (29%)
  other arithmetic  98.2 us (20%)
  blocking collectives  85.9 us (18%)
  local copies, waits for them, and re-layouts  67.5 us (14%)
  matrix products  40.4 us (8%)
  starting transfers between devices  30.8 us (6%)
  between operations  14.2 us (3%)
    all_gather x2, waiting for transfers between devices, entering(): everything = jax.tree.map(lambda part: lax.all_gather(part, axis), x)  87.5 us
    all_gather x2, blocking collectives, entering(): everything = jax.tree.map(lambda part: lax.all_gather(part, axis), x)  42.4 us
    all_gather x1, waiting for transfers between devices, on_device(): lax.all_gather(normed, ('tp', 'dp'), axis=1, tiled=True)  41.1 us
    select_n x32, other arithmetic, turn(): return jax.tree.map(lambda a, b: jnp.where(reached, a, b), new, before)  31.6 us
    all_gather x1, blocking collectives, rows_first(): out = lax.all_gather(both, axis, axis=0, tiled=True)  25.9 us
    all_to_all x1, starting transfers between devices, copy_for_each(): return lax.all_to_all(copies, axis, split_axis=0, concat_axis=0, tiled=True)  24.5 us
    exp x32, other arithmetic, chain_step(): jnp.exp(later[0])[:, None, None] * preceding_entries[1] + later[1]  22.3 us
    all_gather x1, blocking collectives, side_by_side(): lax.all_gather(both, axis, axis=dim, tiled=True)  17.6 us
  transfers between devices with their start and end apart: 7, of which 4 were waited for; matrix products, arithmetic and copies ran while one was open for 22% of the time, Pallas kernels for 0%

commit v1 on v0

v1 whole, which is shorter than its diff:
```python
import functools

import jax
import jax.numpy as jnp
from jax import lax
from jax.experimental import pallas as pl
from jax.experimental.pallas import tpu as pltpu
from jax.sharding import PartitionSpec as P

EPSILON = 1e-06
MESH = pl.DeviceIdType.MESH
F32 = jnp.float32
BF16 = jnp.bfloat16
LANES = 128
NT = (((1,), (1,)), ((), ()))
TN = (((0,), (0,)), ((), ()))


def silu(v):
    return v * (0.5 + 0.5 * jnp.tanh(0.5 * v))


def softplus(v):
    return jnp.maximum(v, 0.0) + jnp.log1p(jnp.exp(-jnp.abs(v)))


def dot(a, b):
    return jnp.dot(a, b, preferred_element_type=F32)


def dot_nt(a, b):
    return lax.dot_general(a, b, NT, preferred_element_type=F32)


def dot_tn(a, b):
    return lax.dot_general(a, b, TN, preferred_element_type=F32)


def remote(src, dst, send, recv, where):
    return pltpu.make_async_remote_copy(
        src_ref=src, dst_ref=dst, send_sem=send, recv_sem=recv, device_id=where, device_id_type=MESH
    )


def aligned(i, n):
    return pl.multiple_of(i * n, n)


def lane_iota(shape):
    return lax.broadcasted_iota(jnp.int32, shape, len(shape) - 1)


def row_iota(shape):
    return lax.broadcasted_iota(jnp.int32, shape, len(shape) - 2)


def expand(cols, first, pair):
    n = cols.shape[0]
    a = first + 2 * pair
    return jnp.where(lane_iota((n, LANES)) < LANES // 2, cols[:, a : a + 1], cols[:, a + 1 : a + 2])


def kernel(
    nz,
    nx,
    latent,
    context,
    shift_w,
    scale_w,
    gate_w,
    og_w,
    sg_w,
    wr_w,
    rd_w,
    out_w,
    cond,
    stepw,
    gain,
    taps,
    bias,
    dlog,
    extra,
    ggain,
    out,
    mw,
    lat,
    ctx,
    hid,
    wog,
    wsg,
    wrd,
    wout,
    pay,
    zrecv,
    msum,
    mods,
    ab,
    rinv,
    rinvc,
    craw,
    cedge,
    raw,
    edge,
    gbuf,
    steprow,
    sbf,
    wbf,
    rbf,
    ldrow,
    strow,
    xrows,
    xt,
    eexp,
    fst,
    fpre,
    bpre,
    bloc,
    stsend,
    strecv,
    ctsend,
    ctrecv,
    dsend,
    drecv,
    dm,
    ed,
    retsend,
    retrecv,
    ybuf,
    nall,
    lsem,
    zs,
    zr,
    ms,
    mr,
    es,
    er,
    ces,
    cer,
    fs,
    fr,
    cs,
    cr,
    ds,
    dr,
    rs,
    rr,
    lats,
    latr,
    gs,
    gr,
    gs2,
    gr2,
    ps,
    pr,
):
    half_rows, width = latent.shape
    span = 2 * half_rows
    nctx = context.shape[0]
    nb = span // LANES
    chan = og_w.shape[1]
    cols = shift_w.shape[1]
    hcols = cols // 2
    po = chan // nz
    nk = nx * 2
    z = lax.axis_index("sp")
    x = lax.axis_index("tp")
    c = lax.axis_index("dp")
    me = x * 2 + c
    up = lax.rem(z + 1, nz)
    down = lax.rem(z + nz - 1, nz)
    right = lax.rem(x + 1, nx)
    left = lax.rem(x + nx - 1, nx)
    own0 = pl.multiple_of(c * half_rows, half_rows)
    oth0 = pl.multiple_of((1 - c) * half_rows, half_rows)

    pairs = [
        (shift_w, mw.at[0]),
        (scale_w, mw.at[1]),
        (gate_w, mw.at[2]),
        (context, ctx),
        (latent, lat.at[pl.ds(own0, half_rows)]),
        (sg_w, wsg),
        (wr_w, wrd.at[:, 0:LANES]),
        (rd_w, wrd.at[:, LANES : 2 * LANES]),
        (og_w, wog),
        (out_w, wout),
    ]
    loads = [pltpu.make_async_copy(s, d, lsem.at[i]) for i, (s, d) in enumerate(pairs)]
    for load in loads:
        load.start()

    barrier = pltpu.get_barrier_semaphore()

    def greet_z(d, _):
        pl.semaphore_signal(barrier, inc=1, device_id={"sp": lax.rem(z + d, nz)}, device_id_type=MESH)
        return 0

    def greet_k(d, _):
        k = lax.rem(me + d, nk)
        pl.semaphore_signal(
            barrier, inc=1, device_id={"tp": k // 2, "dp": lax.rem(k, 2)}, device_id_type=MESH
        )
        return 0

    lax.fori_loop(1, nz, greet_z, 0)
    lax.fori_loop(1, nk, greet_k, 0)

    for i in range(3):
        loads[i].wait()
    zrows = shift_w.shape[0]
    v = cond[:, pl.ds(aligned(z, zrows), zrows)].astype(F32)
    act = silu(v).astype(BF16)
    y = dot(act, mw[0]) + pltpu.roll(dot(act, mw[1]), 2, 0) + pltpu.roll(dot(act, mw[2]), 4, 0)
    pay[...] = jnp.concatenate([y[:, :hcols], y[:, hcols:]], axis=0).astype(BF16)

    pl.semaphore_wait(barrier, nz - 1 + nk - 1)

    def zcast(d):
        return remote(pay, zrecv.at[z], zs.at[d], zr.at[z], {"sp": lax.rem(z + d, nz)})

    def zcast_start(d, _):
        zcast(d).start()
        return 0

    lax.fori_loop(1, nz, zcast_start, 0)
    lat_copy = remote(latent, lat.at[pl.ds(own0, half_rows)], lats, latr, {"dp": 1 - c})
    lat_copy.start()

    def rms_rows(src, base, dst):
        acc = jnp.zeros((16, LANES), F32)
        for j in range(width // 256):
            xx = src[pl.ds(base, 16), j * 256 : (j + 1) * 256].astype(F32)
            sq = xx * xx
            acc = acc + sq[:, :LANES] + sq[:, LANES:]
        s = jnp.sum(acc, axis=1, keepdims=True)
        dst[pl.ds(base, 16), :] = jnp.broadcast_to(lax.rsqrt(s / width + EPSILON), (16, LANES))

    loads[3].wait()

    def rms_ctx(i, _):
        rms_rows(ctx, aligned(i, 16), rinvc)
        return 0

    lax.fori_loop(0, nctx // 16, rms_ctx, 0)
    loads[4].wait()

    def rms_own(i, _):
        rms_rows(lat, pl.multiple_of(own0 + i * 16, 16), rinv)
        return 0

    lax.fori_loop(0, half_rows // 16, rms_own, 0)
    remote(latent, lat.at[pl.ds(oth0, half_rows)], lats, latr, {"dp": 1 - c}).wait_recv()

    def rms_oth(i, _):
        rms_rows(lat, pl.multiple_of(oth0 + i * 16, 16), rinv)
        return 0

    lax.fori_loop(0, half_rows // 16, rms_oth, 0)

    def add_z(d, acc):
        src = lax.rem(z + nz - d, nz)
        remote(pay, zrecv.at[src], zs.at[d], zr.at[src], {"sp": src}).wait_recv()
        return acc + zrecv[src].astype(F32)

    total = lax.fori_loop(1, nz, add_z, pay[...].astype(F32))
    msum[...] = total
    mods[me] = total

    def mcast(d):
        k = lax.rem(me + d, nk)
        return remote(msum, mods.at[me], ms.at[d], mr.at[me], {"tp": k // 2, "dp": lax.rem(k, 2)})

    def mcast_start(d, _):
        mcast(d).start()
        return 0

    lax.fori_loop(1, nk, mcast_start, 0)

    def mcast_take(d, _):
        k = lax.rem(me + nk - d, nk)
        remote(msum, mods.at[k], ms.at[d], mr.at[k], {"tp": k // 2, "dp": lax.rem(k, 2)}).wait_recv()
        return 0

    lax.fori_loop(1, nk, mcast_take, 0)
    for k in range(nk):
        for h in range(2):
            m = mods[k, h * 8 : h * 8 + 8, :]
            at = slice(k * cols + h * hcols, k * cols + (h + 1) * hcols)
            g = gain[:, at]
            ab[0:1, at] = g * (1.0 + m[2:3])
            ab[1:2, at] = m[0:1]
            ab[2:3, at] = g * (1.0 + m[3:4])
            ab[3:4, at] = m[1:2]

    def modulate(src, base, scale_ref, row, dst_base, rows):
        for i in range(rows // 16):
            r = scale_ref[pl.ds(pl.multiple_of(base + i * 16, 16), 16), :]
            for j in range(width // LANES):
                at = slice(j * LANES, (j + 1) * LANES)
                xx = src[pl.ds(pl.multiple_of(base + i * 16, 16), 16), at].astype(F32)
                val = (xx * r) * ab[row : row + 1, at] + ab[row + 1 : row + 2, at]
                hid[pl.ds(pl.multiple_of(dst_base + i * 16, 16), 16), at] = val.astype(BF16)

    def mod_ctx(i, _):
        modulate(ctx, aligned(i, 16), rinvc, 2, pl.multiple_of(span + i * 16, 16), 16)
        return 0

    lax.fori_loop(0, nctx // 16, mod_ctx, 0)

    for i in range(5, 8):
        loads[i].wait()
    hc = hid[span : span + nctx, :]
    craw[8 : 8 + nctx, 0:chan] = dot(hc, wsg[...])
    craw[8 : 8 + nctx, chan : chan + 2 * LANES] = dot(hc, wrd[...])
    cstep = dot_nt(stepw[...], hid[span : span + LANES, :])
    cedge_up = remote(craw.at[nctx : nctx + 8], cedge.at[0], ces.at[0], cer.at[0], {"sp": up})
    cedge_down = remote(craw.at[8:16], cedge.at[1], ces.at[1], cer.at[1], {"sp": down})
    cedge_up.start()
    cedge_down.start()
    loads[8].wait()

    tile = min(256, span)

    def project(row0):
        def mod_lat(i, _):
            at = pl.multiple_of(row0 + i * 32, 32)
            modulate(lat, at, rinv, 0, at, 32)
            return 0

        lax.fori_loop(0, tile // 32, mod_lat, 0)
        h = hid.at[pl.ds(row0, tile)]
        to = pl.multiple_of(row0 + 8, 8)
        raw[pl.ds(to, tile), 0:chan] = dot(h[...], wsg[...])
        raw[pl.ds(to, tile), chan : chan + 2 * LANES] = dot(h[...], wrd[...])
        gbuf[pl.ds(row0, tile), :] = silu(dot(h[...], wog[...]))
        s = dot_nt(stepw[...], h[...])
        for i in range(tile // LANES):
            steprow[row0 // LANES + i] = s[:, i * LANES : (i + 1) * LANES]

    ntiles = span // tile

    def project_ends(i, _):
        project(aligned(i * (ntiles - 1), tile))
        return 0

    lax.fori_loop(0, min(2, ntiles), project_ends, 0)
    edge_up = remote(raw.at[span : span + 8], edge.at[0], es.at[0], er.at[0], {"sp": up})
    edge_down = remote(raw.at[8:16], edge.at[1], es.at[1], er.at[1], {"sp": down})
    edge_up.start()
    edge_down.start()

    def conv(block, at):
        n = block.shape[0]
        mix = (
            taps[0:1, at] * pltpu.roll(block, 1, 0)
            + taps[1:2, at] * block
            + taps[2:3, at] * pltpu.roll(block, n - 1, 0)
        )
        return silu(mix[8 : n - 8])

    first = (z == 0).astype(F32)
    last = (z == nz - 1).astype(F32)
    cedge_up.wait_recv()
    cedge_down.wait_recv()
    craw[7:8, :] = cedge[0, 7:8, :] * (1.0 - first)
    craw[8 + nctx : 9 + nctx, :] = cedge[1, 0:1, :] * (1.0 - last)
    is_fwd = row_iota((8, LANES)) < 4
    lane8 = lane_iota((8, LANES))
    rate = -jnp.exp(dlog[...])
    tri = (
        lax.broadcasted_iota(jnp.int32, (LANES, LANES), 0)
        <= lax.broadcasted_iota(jnp.int32, (LANES, LANES), 1)
    ).astype(F32)

    def cumulate(a):
        return jnp.dot(a, tri, precision=lax.Precision.HIGHEST, preferred_element_type=F32)

    cst = softplus(cstep.astype(BF16).astype(F32) + bias[...])
    cst = jnp.where(lane8 < nctx, cst, 0.0)
    cld = rate * cst
    ccum = cumulate(cld)
    cend = ccum[:, LANES - 1 : LANES]
    cw = jnp.where(is_fwd, jnp.exp(cend - ccum), jnp.exp(ccum - cld)) * cst
    xrows[0, 0:8, :] = cw
    cwt = jnp.transpose(xrows[0:4].reshape(LANES, LANES))[0:nctx, :]
    cblock = [
        conv(craw[0 : nctx + 16, j * LANES : (j + 1) * LANES], slice(j * LANES, (j + 1) * LANES))
        for j in range(chan // LANES + 1)
    ]
    cwr = cblock[-1].astype(BF16)
    for k in range(2):
        for p in range(chan // LANES):
            sc = (cblock[p] * expand(cwt, 4 * k, p)).astype(BF16)
            st = dot_tn(sc, cwr).astype(BF16)
            per = LANES // po
            ctsend[p * per : (p + 1) * per, k] = st.reshape(per, po, LANES)

    def ctcast(d):
        t = lax.rem(z + d, nz)
        return remote(ctsend.at[t], ctrecv.at[z], cs.at[d], cr.at[z], {"sp": t})

    def ctcast_start(d, _):
        ctcast(d).start()
        return 0

    lax.fori_loop(1, nz, ctcast_start, 0)
    ctrecv[z] = ctsend[z]

    def project_rest(i, _):
        project(aligned(i, tile))
        return 0

    lax.fori_loop(1, ntiles - 1, project_rest, 0)

    edge_up.wait_recv()
    edge_down.wait_recv()
    raw[7:8, :] = edge[0, 7:8, :] * (1.0 - first)
    raw[8 + span : 9 + span, :] = edge[1, 0:1, :] * (1.0 - last)

    def conv_block(b, _):
        base = aligned(b, LANES)
        for j in range(chan // LANES + 2):
            at = slice(j * LANES, (j + 1) * LANES)
            val = conv(raw[pl.ds(base, LANES + 16), at], at).astype(BF16)
            if j < chan // LANES:
                sbf[pl.ds(base, LANES), at] = val
            elif j == chan // LANES:
                wbf[pl.ds(base, LANES), :] = val
            else:
                rbf[pl.ds(base, LANES), :] = val
        return 0

    lax.fori_loop(0, nb, conv_block, 0)

    for b in range(nb):
        st = softplus(steprow[b].astype(BF16).astype(F32) + bias[...])
        strow[b] = st
        ldrow[b] = rate * st + extra[:, b * LANES : (b + 1) * LANES]
    cum = cumulate(ldrow[...].reshape(nb * 8, LANES))
    ends = [cum[b * 8 : b * 8 + 8, LANES - 1 : LANES] for b in range(nb)]
    zero = jnp.zeros((8, 1), F32)
    before = [zero]
    for b in range(nb):
        before.append(before[-1] + ends[b])
    after = [zero]
    for b in reversed(range(nb)):
        after.append(after[-1] + ends[b])
    after = after[::-1]
    isf1 = row_iota((8, 1)) < 4
    for b in range(nb):
        cb = cum[b * 8 : b * 8 + 8]
        e = cb - ldrow[b]
        end = ends[b]
        near = jnp.where(is_fwd, cb, end - e)
        xrows[b, 0:8, :] = jnp.where(is_fwd, cb, e)
        xrows[b, 8:16, :] = jnp.where(is_fwd, jnp.exp(end - cb), jnp.exp(e)) * strow[b]
        xrows[b, 16:24, :] = jnp.exp(near)
        xrows[b, 24:32, :] = jnp.exp(near + jnp.where(isf1, before[b], after[b + 1]))
        eexp[b] = jnp.broadcast_to(jnp.exp(end), (8, LANES))
    for g in range(-(-nb // 4)):
        turned = jnp.transpose(xrows[g * 4 : g * 4 + 4].reshape(LANES, LANES))
        for b in range(g * 4, min(nb, g * 4 + 4)):
            xt[b] = turned[:, (b - g * 4) * 32 : (b - g * 4 + 1) * 32]

    npair = chan // LANES
    fst[...] = jnp.zeros_like(fst)

    def decayed(state, b, row):
        lo = eexp[b, row : row + 1, :]
        hi = eexp[b, row + 1 : row + 2, :]
        return jnp.where(row_iota((LANES, LANES)) < LANES // 2, lo, hi) * state

    def forward(b, _):
        base = aligned(b, LANES)
        w = wbf[pl.ds(base, LANES), :]
        cl = xt[b]
        for p in range(npair):
            at = slice(p * LANES, (p + 1) * LANES)
            s = sbf[pl.ds(base, LANES), at].astype(F32)
            fpre[b, at, :] = fst[at, :].astype(BF16)
            fst[at, :] = decayed(fst[at, :], b, 2 * p) + dot_tn((s * expand(cl, 8, p)).astype(BF16), w)
            bloc[b, at, :] = dot_tn((s * expand(cl, 12, p)).astype(BF16), w)
        return 0

    lax.fori_loop(0, nb, forward, 0)
    stsend[:, 0] = fst[...].astype(BF16).reshape(nz, po, LANES)
    fst[...] = jnp.zeros_like(fst)

    def backward(i, _):
        b = nb - 1 - i
        for p in range(npair):
            at = slice(p * LANES, (p + 1) * LANES)
            bpre[b, at, :] = fst[at, :].astype(BF16)
            fst[at, :] = decayed(fst[at, :], b, 4 + 2 * p) + bloc[b, at, :]
        return 0

    lax.fori_loop(0, nb, backward, 0)
    stsend[:, 1] = fst[...].astype(BF16).reshape(nz, po, LANES)
    sub8 = row_iota((8, LANES))
    dsend[...] = jnp.sum(
        jnp.where(lane8 == sub8, before[nb], 0.0) + jnp.where(lane8 == sub8 + 8, cend, 0.0),
        axis=0,
        keepdims=True,
    )

    def stcast(d):
        t = lax.rem(z + d, nz)
        return remote(stsend.at[t], strecv.at[z], fs.at[d], fr.at[z], {"sp": t})

    def dcast(d):
        return remote(dsend, drecv.at[z], ds.at[d], dr.at[z], {"sp": lax.rem(z + d, nz)})

    def stcast_start(d, _):
        dcast(d).start()
        stcast(d).start()
        return 0

    lax.fori_loop(1, nz, stcast_start, 0)
    strecv[z] = stsend[z]
    drecv[z] = dsend[...]

    lower = lax.broadcasted_iota(jnp.int32, (LANES, LANES), 1) <= lax.broadcasted_iota(
        jnp.int32, (LANES, LANES), 0
    )
    upper = lax.broadcasted_iota(jnp.int32, (LANES, LANES), 1) >= lax.broadcasted_iota(
        jnp.int32, (LANES, LANES), 0
    )

    def inside(b, _):
        base = aligned(b, LANES)
        r = rbf[pl.ds(base, LANES), :]
        g = dot_nt(r, wbf[pl.ds(base, LANES), :])
        cl = xt[b]
        for p in range(npair):
            at = slice(p * LANES, (p + 1) * LANES)
            s = sbf[pl.ds(base, LANES), at]
            own = []
            for h in (2 * p, 2 * p + 1):
                arg = jnp.where(
                    lower,
                    cl[:, h : h + 1] - xrows[b, h : h + 1, :],
                    xrows[b, 4 + h : 5 + h, :] - cl[:, 4 + h : 5 + h],
                )
                wgt = jnp.where(lower, strow[b, h : h + 1, :], 0.0) + jnp.where(
                    upper, strow[b, 4 + h : 5 + h, :], 0.0
                )
                own.append(dot((g * jnp.exp(arg) * wgt).astype(BF16), s))
            carried = expand(cl, 16, p) * dot_nt(r, fpre[b, at, :]) + expand(cl, 20, p) * dot_nt(
                r, bpre[b, at, :]
            )
            ybuf[pl.ds(base, LANES), at] = carried + jnp.where(
                lane_iota((LANES, LANES)) < LANES // 2, own[0], own[1]
            )
        return 0

    lax.fori_loop(0, nb, inside, 0)

    def take_states(d, _):
        src = lax.rem(z + nz - d, nz)
        remote(dsend, drecv.at[src], ds.at[d], dr.at[src], {"sp": src}).wait_recv()
        remote(ctsend.at[src], ctrecv.at[src], cs.at[d], cr.at[src], {"sp": src}).wait_recv()
        remote(stsend.at[src], strecv.at[src], fs.at[d], fr.at[src], {"sp": src}).wait_recv()
        return 0

    lax.fori_loop(1, nz, take_states, 0)
    for k in range(nz):
        dm[k : k + 1, :] = drecv[k]
    head = z * po // (LANES // 2)
    dall = dm[...]
    lane_z = lane_iota((nz, LANES))
    for i in range(4):
        col = jnp.sum(jnp.where(lane_z == 4 * i + head, dall, 0.0), axis=1, keepdims=True)
        ed[i] = jnp.exp(jnp.broadcast_to(col, (nz, LANES)))
    state = jnp.zeros((po, LANES), F32)
    for k in range(nz):
        state = ed[2, k : k + 1, :] * state + ctrecv[k, 0].astype(F32)
    for k in range(nz):
        retsend[k, 0] = state.astype(BF16)
        state = ed[0, k : k + 1, :] * state + strecv[k, 0].astype(F32)
    state = jnp.zeros((po, LANES), F32)
    for k in reversed(range(nz)):
        state = ed[3, k : k + 1, :] * state + ctrecv[k, 1].astype(F32)
    for k in reversed(range(nz)):
        retsend[k, 1] = state.astype(BF16)
        state = ed[1, k : k + 1, :] * state + strecv[k, 1].astype(F32)

    def retcast(d):
        t = lax.rem(z + d, nz)
        return remote(retsend.at[t], retrecv.at[z], rs.at[d], rr.at[z], {"sp": t})

    def retcast_start(d, _):
        retcast(d).start()
        return 0

    lax.fori_loop(1, nz, retcast_start, 0)
    retrecv[z] = retsend[z]

    def take_return(d, _):
        src = lax.rem(z + nz - d, nz)
        remote(retsend.at[src], retrecv.at[src], rs.at[d], rr.at[src], {"sp": src}).wait_recv()
        return 0

    lax.fori_loop(1, nz, take_return, 0)

    hrow = LANES // 2

    def piece(k, b):
        return nall.at[k, pl.ds(aligned(b, LANES), LANES)]

    def part(k, b, h):
        return nall.at[k, pl.ds(pl.multiple_of(b * LANES + h * hrow, hrow), hrow)]

    def to_partner(k, i, b):
        return remote(piece(k, b), piece(k, b), ps.at[i, b], pr.at[i, b], {"dp": 1 - c})

    k_left = left * 2 + c
    k_right = right * 2 + c
    k_far = lax.rem(x + 2, nx) * 2 + c

    def own_right(b):
        return remote(piece(me, b), piece(me, b), gs.at[0, b], gr.at[0, b], {"tp": right})

    def own_left(b):
        return remote(piece(me, b), piece(me, b), gs.at[1, b], gr.at[1, b], {"tp": left})

    def relay_right(b):
        return remote(part(k_left, b, 0), part(k_left, b, 0), gs2.at[0, b], gr2.at[0, b], {"tp": right})

    def relay_left(b):
        return remote(part(k_right, b, 1), part(k_right, b, 1), gs2.at[1, b], gr2.at[1, b], {"tp": left})

    def finish(b, _):
        base = aligned(b, LANES)
        r = rbf[pl.ds(base, LANES), :]
        cl = xt[b]
        vals = []
        for p in range(npair):
            at = slice(p * LANES, (p + 1) * LANES)
            per = LANES // po
            f_in = retrecv[p * per : (p + 1) * per, 0].reshape(LANES, LANES)
            b_in = retrecv[p * per : (p + 1) * per, 1].reshape(LANES, LANES)
            yy = (
                ybuf[pl.ds(base, LANES), at]
                + expand(cl, 24, p) * dot_nt(r, f_in)
                + expand(cl, 28, p) * dot_nt(r, b_in)
            )
            vals.append(yy * gbuf[pl.ds(base, LANES), at])
        sq = sum(jnp.sum(a * a, axis=1, keepdims=True) for a in vals)
        inv = lax.rsqrt(sq / chan + EPSILON)
        for p in range(npair):
            at = slice(p * LANES, (p + 1) * LANES)
            nall[me, pl.ds(base, LANES), at] = (vals[p] * inv * ggain[:, at]).astype(BF16)
        own_right(b).start()
        own_left(b).start()
        to_partner(me, 0, b).start()
        return 0

    lax.fori_loop(0, nb, finish, 0)
    loads[9].wait()
    gate = jnp.concatenate([msum[4:5, :], msum[12:13, :]], axis=1)
    out0 = pl.multiple_of(me * cols, cols)

    def collect(i, _):
        @pl.when(i < nb)
        def _():
            remote(piece(k_left, i), piece(k_left, i), gs.at[0, i], gr.at[0, i], {"tp": left}).wait_recv()
            relay_right(i).start()
            to_partner(k_left, 1, i).start()
            remote(piece(k_right, i), piece(k_right, i), gs.at[1, i], gr.at[1, i], {"tp": right}).wait_recv()
            relay_left(i).start()
            to_partner(k_right, 2, i).start()

        @pl.when(jnp.logical_and(i >= 1, i <= nb))
        def _():
            b = i - 1
            for h in range(2):
                remote(part(k_far, b, h), part(k_far, b, h), gs2.at[h, b], gr2.at[h, b], {"tp": left}).wait_recv()
            to_partner(k_far, 3, b).start()

        @pl.when(i >= 2)
        def _():
            b = i - 2
            flip = 1 - 2 * c
            for n, k in enumerate((me, k_left, k_right, k_far)):
                to_partner(k + flip, n, b).wait_recv()
            base = aligned(b, LANES)
            acc = jnp.zeros((LANES, cols), F32)
            for k in range(nk):
                acc = acc + dot(nall[k, pl.ds(base, LANES), :], wout[k * chan : (k + 1) * chan, :])
            res = lat[pl.ds(base, LANES), pl.ds(out0, cols)].astype(F32)
            out[pl.ds(base, LANES), :] = (res + gate * acc).astype(BF16)

        return 0

    lax.fori_loop(0, nb + 2, collect, 0)

    lat_copy.wait_send()
    cedge_up.wait_send()
    cedge_down.wait_send()
    edge_up.wait_send()
    edge_down.wait_send()

    def drain_z(d, _):
        zcast(d).wait_send()
        ctcast(d).wait_send()
        stcast(d).wait_send()
        dcast(d).wait_send()
        retcast(d).wait_send()
        return 0

    lax.fori_loop(1, nz, drain_z, 0)

    def drain_k(d, _):
        mcast(d).wait_send()
        return 0

    lax.fori_loop(1, nk, drain_k, 0)

    def drain_b(b, _):
        own_right(b).wait_send()
        own_left(b).wait_send()
        relay_right(b).wait_send()
        relay_left(b).wait_send()
        for i in range(4):
            to_partner(me, i, b).wait_send()
        return 0

    lax.fori_loop(0, nb, drain_b, 0)


def on_device(
    latent,
    context,
    condition,
    context_condition,
    shift_weight,
    scale_weight,
    gate_weight,
    norm_gain,
    out_gate_weight,
    signal_weight,
    writer_weight,
    reader_matrix,
    step_weight,
    signal_taps,
    writer_taps,
    reader_taps,
    step_bias,
    decay_log,
    decay_extra,
    group_gain,
    output_weight,
):
    nz, nx = lax.axis_size("sp"), lax.axis_size("tp")
    half_rows, width = latent.shape
    span, nctx = 2 * half_rows, context.shape[0]
    chan, cols = out_gate_weight.shape[1], shift_weight.shape[1]
    nb, nk, po = span // LANES, 2 * nx, chan // nz
    full = chan + 2 * LANES
    rows8 = 2 * step_bias.shape[1]
    cond = jnp.concatenate(
        [condition[None], context_condition[None], jnp.zeros((6, width), BF16)], axis=0
    )
    stepw = jnp.transpose(step_weight, (0, 2, 1)).reshape(rows8, width)
    taps = jnp.concatenate([signal_taps, writer_taps, reader_taps], axis=1)
    hbm = pl.BlockSpec(memory_space=pl.ANY)
    vmem = pl.BlockSpec(memory_space=pltpu.VMEM)
    dma = pltpu.SemaphoreType.DMA
    scratch = [
        ((3, *shift_weight.shape), BF16),
        ((span, width), BF16),
        ((nctx, width), BF16),
        ((span + LANES, width), BF16),
        ((width, chan), BF16),
        ((width, chan), BF16),
        ((width, 2 * LANES), BF16),
        (output_weight.shape, BF16),
        ((16, cols // 2), BF16),
        ((nz, 16, cols // 2), BF16),
        ((16, cols // 2), F32),
        ((nk, 16, cols // 2), F32),
        ((8, width), F32),
        ((span, LANES), F32),
        ((nctx, LANES), F32),
        ((nctx + 16, full), F32),
        ((2, 8, full), F32),
        ((span + 16, full), F32),
        ((2, 8, full), F32),
        ((span, chan), F32),
        ((nb, 8, LANES), F32),
        ((span, chan), BF16),
        ((span, LANES), BF16),
        ((span, LANES), BF16),
        ((nb, 8, LANES), F32),
        ((nb, 8, LANES), F32),
        ((-(-nb // 4) * 4, 32, LANES), F32),
        ((nb, LANES, 32), F32),
        ((nb, 8, LANES), F32),
        ((chan, LANES), F32),
        ((nb, chan, LANES), BF16),
        ((nb, chan, LANES), BF16),
        ((nb, chan, LANES), F32),
        ((nz, 2, po, LANES), BF16),
        ((nz, 2, po, LANES), BF16),
        ((nz, 2, po, LANES), BF16),
        ((nz, 2, po, LANES), BF16),
        ((1, LANES), F32),
        ((nz, 1, LANES), F32),
        ((nz, LANES), F32),
        ((4, nz, LANES), F32),
        ((nz, 2, po, LANES), BF16),
        ((nz, 2, po, LANES), BF16),
        ((span, chan), F32),
        ((nk, span, chan), BF16),
    ]
    sems = [
        (10,),
        (nz,),
        (nz,),
        (nk,),
        (nk,),
        (2,),
        (2,),
        (2,),
        (2,),
        (nz,),
        (nz,),
        (nz,),
        (nz,),
        (nz,),
        (nz,),
        (nz,),
        (nz,),
        None,
        None,
        (2, nb),
        (2, nb),
        (2, nb),
        (2, nb),
        (4, nb),
        (4, nb),
    ]
    return pl.pallas_call(
        functools.partial(kernel, nz, nx),
        out_shape=jax.ShapeDtypeStruct((span, cols), BF16),
        in_specs=[hbm] * 10 + [vmem] * 8,
        out_specs=vmem,
        scratch_shapes=[pltpu.VMEM(s, t) for s, t in scratch]
        + [dma if s is None else dma(s) for s in sems],
        compiler_params=pltpu.CompilerParams(
            collective_id=0, has_side_effects=True, vmem_limit_bytes=60 * 1024 * 1024
        ),
        name="mixing",
    )(
        latent,
        context,
        shift_weight,
        scale_weight,
        gate_weight,
        out_gate_weight,
        signal_weight,
        writer_weight,
        reader_matrix,
        output_weight,
        cond,
        stepw,
        norm_gain.reshape(1, width),
        taps,
        step_bias.reshape(rows8, 1),
        decay_log.reshape(rows8, 1),
        decay_extra.reshape(rows8, span),
        group_gain.reshape(1, chan),
    )


def solution(mesh):
    in_specs = (
        P(("grp", "sp", "dp"), None),
        P(("grp", "sp"), None),
        P("grp"),
        P(),
        P("sp", ("tp", "dp")),
        P("sp", ("tp", "dp")),
        P("sp", ("tp", "dp")),
        P(),
        P(None, ("tp", "dp")),
        P(None, ("tp", "dp")),
        P(None, ("tp", "dp")),
        P(None, ("tp", "dp")),
        P(None, None, ("tp", "dp")),
        P(None, ("tp", "dp")),
        P(None, ("tp", "dp")),
        P(None, ("tp", "dp")),
        P(None, ("tp", "dp")),
        P(None, ("tp", "dp")),
        P(None, ("tp", "dp"), ("grp", "sp")),
        P(("tp", "dp")),
        P(None, ("tp", "dp")),
    )
    out_specs = P(("grp", "sp"), ("tp", "dp"))
    return jax.shard_map(
        on_device, mesh=mesh, in_specs=in_specs, out_specs=out_specs, check_vma=False
    )
```

time: 482 us -> 116 us (0.24)
  waiting for transfers between devices: 140 us -> 0 us
  Pallas kernels: 0 us -> 105 us
  other arithmetic: 98.2 us -> 2.02 us
  blocking collectives: 85.9 us -> 0 us
  local copies, waits for them, and re-layouts: 67.5 us -> 9.07 us
  matrix products: 40.4 us -> 0 us
  starting transfers between devices: 30.8 us -> 0 us
  between operations: 14.2 us -> 0.02 us
    all_gather x4 -> x0, waiting for transfers between devices: 129 us -> none  [the longest x2 87.5 us: entering(): everything = jax.tree.map(lambda part: lax.all_gather(part, axis), x)]
    pallas_call x0 -> x1, Pallas kernels: none -> 105 us  [on_device(): pl.pallas_call(functools.partial(kernel, nz, nx), out_shape=jax.ShapeDtyp...]
    all_gather x4 -> x0, blocking collectives: 85.9 us -> none  [the longest x2 42.4 us: entering(): everything = jax.tree.map(lambda part: lax.all_gather(part, axis), x)]
    dot_general x25 -> x0, matrix products: 40.4 us -> none  [the longest x1 5.52 us: on_device(): jnp.dot(hidden, out_gate_weight, preferred_element_type=jnp.float32)]
    select_n x33 -> x0, other arithmetic: 31.7 us -> none  [the longest x32 31.6 us: turn(): return jax.tree.map(lambda a, b: jnp.where(reached, a, b), new, before)]
    exp x34 -> x0, other arithmetic: 25.8 us -> none  [the longest x32 22.3 us: chain_step(): jnp.exp(later[0])[:, None, None] * preceding_entries[1] + later[1]]
    all_to_all x1 -> x0, starting transfers between devices: 24.5 us -> none  [copy_for_each(): return lax.all_to_all(copies, axis, split_axis=0, concat_axis=0, tiled=True)]
    another operation x15 -> x0, local copies, waits for them, and re-layouts: 15.1 us -> none
  transfers between devices with their start and end apart: 7 -> 0, of which waited for: 4 -> 0; matrix products, arithmetic and copies ran while one was open for 22% -> 0% of each run, Pallas kernels for 0% -> 0%
where the time goes in v1:
time: 116 us
  Pallas kernels  105 us (91%)
  local copies, waits for them, and re-layouts  9.07 us (8%)
  other arithmetic  2.02 us (2%)
    pallas_call x1, Pallas kernels, on_device(): pl.pallas_call(functools.partial(kernel, nz, nx), out_shape=jax.ShapeDtyp...  105 us

profile of v1, /device:TPU:33, one launch (start us, length us, event | category | flops | bytes accessed | tf_op | source)
XLA Modules:
  0.0 115.8 jit_solution(5458802291369475403)
XLA Ops:
  0.0 0.1 pad.5.clone
  0.1 1.3 %reshape.24.bias = f32[8,1]{1,0:T(8,128)} reshape(f32[2,4]{1,0:T(2,128)} %param.37) | data formatting | bytes 64 | tf_op jit(solution)/shard_map/reshape | solution.py:869
  1.4 1.3 %reshape.25.dlog = f32[8,1]{1,0:T(8,128)} reshape(f32[2,4]{1,0:T(2,128)} %param.38) | data formatting | bytes 64 | tf_op jit(solution)/shard_map/reshape | solution.py:870
  2.8 1.3 %pad_maximum_fusion.taps = f32[3,512]{1,0:T(4,128)} fusion(f32[3,128]{1,0:T(4,128)} %param.36, f32[3,128]{1,0:T(4,128)} %param.35, f32[3,256]{1,0:T(4,128)} %param.34), kind=kLoop, calls=%fused_computation.1 | loop fusion | flops 3072 | bytes 12288 | tf_op jit(solution)/shard_map/concatenate | solution.py:765
  4.1 0.7 broadcast_in_dim.9
  4.8 0.7 broadcast_in_dim.10
  5.5 1.4 %reshape.22.extra = f32[8,768]{1,0:T(8,128)} reshape(f32[2,4,768]{2,1,0:T(4,128)} %param.39) | data formatting | bytes 49152 | tf_op jit(solution)/shard_map/reshape | solution.py:871
  6.9 0.7 maximum_maximum_fusion.cond
  7.6 1.5 %reshape.18.stepw = bf16[8,4096]{1,0:T(8,128)(2,1)} reshape(bf16[2,4,4096]{2,1,0:T(4,128)(2,1)} %bitcast.3) | data formatting | bytes 131072 | tf_op jit(solution)/shard_map/reshape | solution.py:764
  9.0 104.7 %mixing.1 = bf16[768,512]{1,0:T(8,128)(2,1)} custom-call(bf16[384,4096]{1,0:T(8,128)(2,1)} %latent.1, bf16[32,4096]{1,0:T(8,128)(2,1)} %context.1, bf16[256,512]{1,0:T(8,128)(2,1)} %shift_w.1, bf16[256,512]{1,0:T(8,128)(2,1)} %scale_w.1, bf16[256,512]{1,0:T(8,128)(2,1)} %gate_w.1, bf16[4096,256]{1,0:T(8,128)(2,1)} %og_w.1, bf16[4096,256]{1,0:T(8,128)(2,1)} %sg_w.1, ...), custom_call_target="tpu_custom_call" | custom-call | tf_op jit(solution)/shard_map/mixing/pallas_call | solution.py:843
  113.8 2.1 %copy.25 = bf16[768,512]{1,0:T(8,128)(2,1)} copy(bf16[768,512]{1,0:T(8,128)(2,1)} %mixing.1) | data formatting | bytes 1572864
  (1 shorter events, 0.0 us)

commit v2 on v1

v2 whole, which is shorter than its diff:
```python
import functools

import jax
import jax.numpy as jnp
from jax import lax
from jax.experimental import pallas as pl
from jax.experimental.pallas import tpu as pltpu
from jax.sharding import PartitionSpec as P

EPSILON = 1e-06
OVERLAP = True
MESH = pl.DeviceIdType.MESH
F32 = jnp.float32
BF16 = jnp.bfloat16
LANES = 128
NT = (((1,), (1,)), ((), ()))
TN = (((0,), (0,)), ((), ()))


def silu(v):
    return v * (0.5 + 0.5 * jnp.tanh(0.5 * v))


def softplus(v):
    return jnp.maximum(v, 0.0) + jnp.log1p(jnp.exp(-jnp.abs(v)))


def dot(a, b):
    return jnp.dot(a, b, preferred_element_type=F32)


def dot_nt(a, b):
    return lax.dot_general(a, b, NT, preferred_element_type=F32)


def dot_tn(a, b):
    return lax.dot_general(a, b, TN, preferred_element_type=F32)


def remote(src, dst, send, recv, where):
    return pltpu.make_async_remote_copy(
        src_ref=src, dst_ref=dst, send_sem=send, recv_sem=recv, device_id=where, device_id_type=MESH
    )


def aligned(i, n):
    return pl.multiple_of(i * n, n)


def lane_iota(shape):
    return lax.broadcasted_iota(jnp.int32, shape, len(shape) - 1)


def row_iota(shape):
    return lax.broadcasted_iota(jnp.int32, shape, len(shape) - 2)


def expand(cols, first, pair):
    n = cols.shape[0]
    a = first + 2 * pair
    return jnp.where(lane_iota((n, LANES)) < LANES // 2, cols[:, a : a + 1], cols[:, a + 1 : a + 2])


def kernel(
    nz,
    nx,
    latent,
    context,
    shift_w,
    scale_w,
    gate_w,
    og_w,
    sg_w,
    wr_w,
    rd_w,
    out_w,
    cond,
    ctx_cond,
    stepw_in,
    gain,
    signal_taps,
    writer_taps,
    reader_taps,
    bias_in,
    dlog_in,
    extra,
    ggain,
    out,
    condrow,
    taps,
    mw,
    lat,
    ctx,
    hid0,
    hid1,
    hid2,
    acc,
    wog,
    wsg,
    wsw,
    wrd,
    wout,
    pay,
    zrecv,
    gpay,
    grecv,
    msum,
    mods,
    ab,
    rinv,
    rinvc,
    craw,
    cedge,
    cstepc,
    raw,
    edge,
    rraw,
    redge,
    rsend,
    gbuf,
    stepc,
    sbf,
    wbf,
    rbf,
    ldrow,
    strow,
    xrows,
    xt,
    eexp,
    loc,
    fpre,
    bpre,
    fsend,
    frecv,
    bsend,
    brecv,
    ctsend,
    ctrecv,
    dsend,
    drecv,
    dm,
    ed,
    fback,
    fin,
    bback,
    bin_,
    ybuf,
    nall,
    oacc,
    obuf,
    lsem,
    zs,
    zr,
    ms,
    mr,
    es,
    er,
    res,
    rer,
    ces,
    cer,
    gzs,
    gzr,
    fs,
    fr,
    bs,
    br,
    cs,
    cr,
    ds,
    dr,
    rs,
    rr,
    rbs,
    rbr,
    lats,
    latr,
    gs,
    gr,
    gs2,
    gr2,
    ps,
    pr,
    osem,
):
    scopes = []

    def phase(name):
        if scopes:
            scopes.pop().__exit__(None, None, None)
        if name:
            scopes.append(jax.named_scope(name))
            scopes[-1].__enter__()

    phase("p_start")
    half_rows, width = latent.shape
    span = 2 * half_rows
    nctx = context.shape[0]
    nb = span // LANES
    chan = og_w.shape[1]
    cols = shift_w.shape[1]
    po = chan // nz
    nk = nx * 2
    z = lax.axis_index("sp")
    x = lax.axis_index("tp")
    c = lax.axis_index("dp")
    me = x * 2 + c
    up = lax.rem(z + 1, nz)
    down = lax.rem(z + nz - 1, nz)
    right = lax.rem(x + 1, nx)
    left = lax.rem(x + nx - 1, nx)
    own0 = pl.multiple_of(c * half_rows, half_rows)
    oth0 = pl.multiple_of((1 - c) * half_rows, half_rows)

    pairs = [
        (shift_w, mw.at[0]),
        (scale_w, mw.at[1]),
        (gate_w, mw.at[2]),
        (context, ctx),
        (latent, lat.at[pl.ds(own0, half_rows)]),
        (sg_w, wsg),
        (wr_w, wsw.at[:, 0:LANES]),
        (rd_w, wrd),
        (og_w, wog),
        (out_w, wout),
    ]
    loads = [pltpu.make_async_copy(s, d, lsem.at[i]) for i, (s, d) in enumerate(pairs)]
    for load in loads:
        load.start()

    barrier = pltpu.get_barrier_semaphore()

    def greet_z(d, _):
        pl.semaphore_signal(barrier, inc=1, device_id={"sp": lax.rem(z + d, nz)}, device_id_type=MESH)
        return 0

    def greet_k(d, _):
        k = lax.rem(me + d, nk)
        pl.semaphore_signal(
            barrier, inc=1, device_id={"tp": k // 2, "dp": lax.rem(k, 2)}, device_id_type=MESH
        )
        return 0

    lax.fori_loop(1, nz, greet_z, 0)
    lax.fori_loop(1, nk, greet_k, 0)

    phase("p_matvec")
    zrows = shift_w.shape[0]
    condrow[...] = jnp.zeros_like(condrow)
    condrow[0:1, :] = cond[...].astype(F32).reshape(1, width)
    condrow[1:2, :] = ctx_cond[...].astype(F32).reshape(1, width)
    act = silu(condrow[:, pl.ds(aligned(z, zrows), zrows)]).astype(BF16)
    for i in range(3):
        loads[i].wait()
    y = dot(act, mw[0]) + pltpu.roll(dot(act, mw[1]), 2, 0)
    pay[...] = jnp.concatenate(
        [y[0:4, j * LANES : (j + 1) * LANES] for j in range(cols // LANES)], axis=0
    ).astype(BF16)
    gpay[...] = dot(act, mw[2])[0:1, :]

    phase("p_barrier")
    pl.semaphore_wait(barrier, nz - 1 + nk - 1)
    phase("p_zcast")

    def zcast(d):
        return remote(pay, zrecv.at[z], zs.at[d], zr.at[z], {"sp": lax.rem(z + d, nz)})

    def zcast_start(d, _):
        zcast(d).start()
        return 0

    lax.fori_loop(1, nz, zcast_start, 0)
    lat_copy = remote(latent, lat.at[pl.ds(own0, half_rows)], lats, latr, {"dp": 1 - c})
    lat_copy.start()

    taps[:, 0:chan] = signal_taps[...]
    taps[:, chan : chan + LANES] = writer_taps[...]
    taps[:, chan + LANES : chan + 2 * LANES] = reader_taps[...]
    sub4 = lax.broadcasted_iota(jnp.int32, (8, 4), 0)
    pick4 = lax.broadcasted_iota(jnp.int32, (8, 4), 1) == lax.rem(sub4, 4)

    def column(ref):
        both = jnp.where(sub4 < 4, ref[0:1, :], ref[1:2, :])
        return jnp.sum(jnp.where(pick4, both, 0.0), axis=1, keepdims=True)

    bias = column(bias_in)
    rate = -jnp.exp(column(dlog_in))

    def step_cols(i, _):
        at = pl.ds(aligned(i, LANES), LANES)
        rows = [
            stepw_in[0, :, at].astype(F32),
            stepw_in[1, :, at].astype(F32),
            jnp.zeros((LANES - 8, LANES), F32),
        ]
        wsw[at, LANES : 2 * LANES] = jnp.transpose(jnp.concatenate(rows, axis=0)).astype(BF16)

    def step_cols4(i, _):
        for n in range(4):
            step_cols(i * 4 + n, 0)
        return 0

    lax.fori_loop(0, width // LANES // 4, step_cols4, 0)

    def rms_rows(src, base, rows, dst):
        at = pl.ds(base, rows)
        sums = jnp.zeros((rows, LANES), F32)
        for j in range(width // LANES):
            xx = src[at, j * LANES : (j + 1) * LANES].astype(F32)
            sums = sums + xx * xx
        total = jnp.sum(sums, axis=1, keepdims=True)
        dst[at, :] = jnp.broadcast_to(lax.rsqrt(total / width + EPSILON), (rows, LANES))

    loads[3].wait()
    rms_rows(ctx, 0, nctx, rinvc)
    loads[4].wait()
    rblock = 64

    def rms_own(i, _):
        rms_rows(lat, pl.multiple_of(own0 + i * rblock, rblock), rblock, rinv)
        return 0

    lax.fori_loop(0, half_rows // rblock, rms_own, 0)
    remote(latent, lat.at[pl.ds(oth0, half_rows)], lats, latr, {"dp": 1 - c}).wait_recv()

    def rms_oth(i, _):
        rms_rows(lat, pl.multiple_of(oth0 + i * rblock, rblock), rblock, rinv)
        return 0

    lax.fori_loop(0, half_rows // rblock, rms_oth, 0)

    phase("p_zwait")
    def add_z(d, acc):
        src = lax.rem(z + nz - d, nz)
        remote(pay, zrecv.at[src], zs.at[d], zr.at[src], {"sp": src}).wait_recv()
        return acc + zrecv[src].astype(F32)

    total = lax.fori_loop(1, nz, add_z, pay[...].astype(F32))
    msum[...] = total
    mods[me] = total

    def mcast(d):
        k = lax.rem(me + d, nk)
        return remote(msum, mods.at[me], ms.at[d], mr.at[me], {"tp": k // 2, "dp": lax.rem(k, 2)})

    def mcast_start(d, _):
        mcast(d).start()
        return 0

    lax.fori_loop(1, nk, mcast_start, 0)
    phase("p_mwait")

    def gcast(d):
        return remote(gpay, grecv.at[z], gzs.at[d], gzr.at[z], {"sp": lax.rem(z + d, nz)})

    def gcast_start(d, _):
        gcast(d).start()
        return 0

    lax.fori_loop(1, nz, gcast_start, 0)

    def mcast_take(d, _):
        k = lax.rem(me + nk - d, nk)
        remote(msum, mods.at[k], ms.at[d], mr.at[k], {"tp": k // 2, "dp": lax.rem(k, 2)}).wait_recv()
        return 0

    lax.fori_loop(1, nk, mcast_take, 0)
    for k in range(nk):
        for j in range(cols // LANES):
            m = mods[k, j * 4 : j * 4 + 4, :]
            at = slice(k * cols + j * LANES, k * cols + (j + 1) * LANES)
            g = gain[:, at]
            ab[0:1, at] = g * (1.0 + m[2:3])
            ab[1:2, at] = m[0:1]
            ab[2:3, at] = g * (1.0 + m[3:4])
            ab[3:4, at] = m[1:2]
    phase("p_mod0")
    tile = hid1.shape[0]
    both = chan + LANES
    piece_cols = 512
    steps = width // piece_cols

    def modulate(src, base, rows, inv, row, dst, to, kk):
        for j in range(piece_cols // LANES):
            start = kk * piece_cols + j * LANES
            at = pl.ds(start if isinstance(start, int) else pl.multiple_of(start, LANES), LANES)
            up_row = ab[row : row + 1, at]
            add_row = ab[row + 1 : row + 2, at]
            for i in range(rows // 32):
                r = inv[base + i * 32 : base + (i + 1) * 32, :]
                xx = src[base + i * 32 : base + (i + 1) * 32, at].astype(F32)
                dst[to + i * 32 : to + (i + 1) * 32, at] = (xx * r * up_row + add_row).astype(BF16)

    def multiply(h):
        rows = h.shape[0]
        acc[0:rows, 0:chan] = dot(h[...], wsg[...])
        acc[0:rows, chan : chan + 2 * LANES] = dot(h[...], wsw[...])

    def modulate_tile(t, dst):
        if OVERLAP:
            for kk in range(steps):
                modulate(lat, t * tile, tile, rinv, 0, dst, 0, kk)
        else:

            def turn(kk, _):
                modulate(lat, t * tile, tile, rinv, 0, dst, 0, kk)
                return 0

            lax.fori_loop(0, steps, turn, 0)

    def mod_first(kk, _):
        modulate(ctx, 0, nctx, rinvc, 2, hid0, 0, kk)
        modulate(lat, 0, tile, rinv, 0, hid0, nctx, kk)
        return 0

    lax.fori_loop(0, steps, mod_first, 0)
    for i in range(5, 7):
        loads[i].wait()
    phase("p_dots0")
    multiply(hid0)
    modulate_tile(2, hid2)
    craw[8 : 8 + nctx, :] = acc[0:nctx, 0:both]
    cstepc[0:nctx, :] = acc[0:nctx, both : both + LANES]
    raw[8 : 8 + tile, :] = acc[nctx : nctx + tile, 0:both]
    stepc[0:tile, :] = acc[nctx : nctx + tile, both : both + LANES]
    cedge_up = remote(craw.at[nctx : nctx + 8], cedge.at[0], ces.at[0], cer.at[0], {"sp": up})
    cedge_down = remote(craw.at[8:16], cedge.at[1], ces.at[1], cer.at[1], {"sp": down})
    cedge_up.start()
    cedge_down.start()
    phase("p_dots2")
    multiply(hid2)
    modulate_tile(1, hid1)
    raw[8 + 2 * tile : 8 + 3 * tile, :] = acc[0:tile, 0:both]
    stepc[2 * tile : 3 * tile, :] = acc[0:tile, both : both + LANES]
    edge_up = remote(raw.at[span : span + 8], edge.at[0], es.at[0], er.at[0], {"sp": up})
    edge_down = remote(raw.at[8:16], edge.at[1], es.at[1], er.at[1], {"sp": down})
    edge_up.start()
    edge_down.start()
    loads[7].wait()
    ends = jnp.concatenate([hid0[nctx : nctx + 16, :], hid2[tile - 16 : tile, :]], axis=0)
    rends = dot(ends, wrd[...])
    rsend[0] = rends[24:32, :]
    rsend[1] = rends[0:8, :]
    redge_up = remote(rsend.at[0], redge.at[0], res.at[0], rer.at[0], {"sp": up})
    redge_down = remote(rsend.at[1], redge.at[1], res.at[1], rer.at[1], {"sp": down})
    redge_up.start()
    redge_down.start()
    phase("p_dots1")
    multiply(hid1)
    raw[8 + tile : 8 + 2 * tile, :] = acc[0:tile, 0:both]
    stepc[tile : 2 * tile, :] = acc[0:tile, both : both + LANES]

    phase("p_ctxstate")
    def conv(block, at):
        n = block.shape[0]
        mix = (
            taps[0:1, at] * pltpu.roll(block, 1, 0)
            + taps[1:2, at] * block
            + taps[2:3, at] * pltpu.roll(block, n - 1, 0)
        )
        return silu(mix[8 : n - 8])

    first = (z == 0).astype(F32)
    last = (z == nz - 1).astype(F32)
    cedge_up.wait_recv()
    cedge_down.wait_recv()
    craw[7:8, :] = cedge[0, 7:8, :] * (1.0 - first)
    craw[8 + nctx : 9 + nctx, :] = cedge[1, 0:1, :] * (1.0 - last)
    is_fwd = row_iota((8, LANES)) < 4
    lane8 = lane_iota((8, LANES))
    tri = (
        lax.broadcasted_iota(jnp.int32, (LANES, LANES), 0)
        <= lax.broadcasted_iota(jnp.int32, (LANES, LANES), 1)
    ).astype(F32)

    def cumulate(a):
        return jnp.dot(a, tri, precision=lax.Precision.HIGHEST, preferred_element_type=F32)

    cstep = jnp.transpose(cstepc[...])[0:8, :]
    cst = softplus(cstep.astype(BF16).astype(F32) + bias)
    cst = jnp.where(lane8 < nctx, cst, 0.0)
    cld = rate * cst
    ccum = cumulate(cld)
    cend = ccum[:, LANES - 1 : LANES]
    cw = jnp.where(is_fwd, jnp.exp(cend - ccum), jnp.exp(ccum - cld)) * cst
    xrows[0, 0:8, :] = cw
    cwt = jnp.transpose(xrows[0:4].reshape(LANES, LANES))[0:nctx, :]
    cblock = [
        conv(craw[0 : nctx + 16, j * LANES : (j + 1) * LANES], slice(j * LANES, (j + 1) * LANES))
        for j in range(chan // LANES + 1)
    ]
    cwr = cblock[-1].astype(BF16)
    for k in range(2):
        for p in range(chan // LANES):
            sc = (cblock[p] * expand(cwt, 4 * k, p)).astype(BF16)
            st = dot_tn(sc, cwr).astype(BF16)
            per = LANES // po
            ctsend[p * per : (p + 1) * per, k] = st.reshape(per, po, LANES)

    def ctcast(d):
        t = lax.rem(z + d, nz)
        return remote(ctsend.at[t], ctrecv.at[z], cs.at[d], cr.at[z], {"sp": t})

    def ctcast_start(d, _):
        ctcast(d).start()
        return 0

    lax.fori_loop(1, nz, ctcast_start, 0)
    ctrecv[z] = ctsend[z]
    phase("p_edge")
    edge_up.wait_recv()
    edge_down.wait_recv()
    raw[7:8, :] = edge[0, 7:8, :] * (1.0 - first)
    raw[8 + span : 9 + span, :] = edge[1, 0:1, :] * (1.0 - last)

    phase("p_conv")

    def conv_block(b, _):
        base = aligned(b, LANES)
        for j in range(chan // LANES + 1):
            at = slice(j * LANES, (j + 1) * LANES)
            val = conv(raw[pl.ds(base, LANES + 16), at], at).astype(BF16)
            if j < chan // LANES:
                sbf[pl.ds(base, LANES), at] = val
            else:
                wbf[pl.ds(base, LANES), :] = val
        return 0

    lax.fori_loop(0, nb, conv_block, 0)

    phase("p_rows")
    for b in range(nb):
        turned = jnp.transpose(stepc[b * LANES : (b + 1) * LANES, :])[0:8, :]
        st = softplus(turned.astype(BF16).astype(F32) + bias)
        strow[b] = st
        ldrow[b] = rate * st + jnp.concatenate(
            [extra[0, :, b * LANES : (b + 1) * LANES], extra[1, :, b * LANES : (b + 1) * LANES]], axis=0
        )
    cum = cumulate(ldrow[...].reshape(nb * 8, LANES))
    ends = [cum[b * 8 : b * 8 + 8, LANES - 1 : LANES] for b in range(nb)]
    zero = jnp.zeros((8, 1), F32)
    before = [zero]
    for b in range(nb):
        before.append(before[-1] + ends[b])
    after = [zero]
    for b in reversed(range(nb)):
        after.append(after[-1] + ends[b])
    after = after[::-1]
    isf1 = row_iota((8, 1)) < 4
    for b in range(nb):
        cb = cum[b * 8 : b * 8 + 8]
        e = cb - ldrow[b]
        end = ends[b]
        near = jnp.where(is_fwd, cb, end - e)
        xrows[b, 0:8, :] = jnp.where(is_fwd, cb, e)
        xrows[b, 8:16, :] = jnp.where(is_fwd, jnp.exp(end - cb), jnp.exp(e)) * strow[b]
        xrows[b, 16:24, :] = jnp.exp(near)
        xrows[b, 24:32, :] = jnp.exp(near + jnp.where(isf1, before[b], after[b + 1]))
        eexp[b] = jnp.broadcast_to(jnp.exp(end), (8, LANES))
    for g in range(-(-nb // 4)):
        turned = jnp.transpose(xrows[g * 4 : g * 4 + 4].reshape(LANES, LANES))
        for b in range(g * 4, min(nb, g * 4 + 4)):
            xt[b] = turned[:, (b - g * 4) * 32 : (b - g * 4 + 1) * 32]

    phase("p_states")
    npair = chan // LANES
    def decayed(state, b, row):
        lo = eexp[b, row : row + 1, :]
        hi = eexp[b, row + 1 : row + 2, :]
        return jnp.where(row_iota((LANES, LANES)) < LANES // 2, lo, hi) * state

    sub8 = row_iota((8, LANES))
    dsend[...] = jnp.sum(
        jnp.where(lane8 == sub8, before[nb], 0.0) + jnp.where(lane8 == sub8 + 8, cend, 0.0),
        axis=0,
        keepdims=True,
    )

    def dcast(d):
        return remote(dsend, drecv.at[z], ds.at[d], dr.at[z], {"sp": lax.rem(z + d, nz)})

    def fcast(d):
        t = lax.rem(z + d, nz)
        return remote(fsend.at[t], frecv.at[z], fs.at[d], fr.at[z], {"sp": t})

    def bcast(d):
        t = lax.rem(z + d, nz)
        return remote(bsend.at[t], brecv.at[z], bs.at[d], br.at[z], {"sp": t})

    def dcast_start(d, _):
        dcast(d).start()
        return 0

    def fcast_start(d, _):
        fcast(d).start()
        return 0

    def bcast_start(d, _):
        bcast(d).start()
        return 0

    lax.fori_loop(1, nz, dcast_start, 0)
    drecv[z] = dsend[...]

    def contribute(first):
        for b in range(nb):
            base = b * LANES
            w = wbf[base : base + LANES, :]
            cl = xt[b]
            for p in range(npair):
                at = slice(p * LANES, (p + 1) * LANES)
                v = sbf[base : base + LANES, at].astype(F32) * expand(cl, first, p)
                loc[b, at, :] = dot_tn(v.astype(BF16), w)

    def chain(order, row, before_ref, send_ref):
        per = LANES // po
        for p in range(npair):
            at = slice(p * LANES, (p + 1) * LANES)
            state = jnp.zeros((LANES, LANES), F32)
            for b in order:
                before_ref[b, at, :] = state.astype(BF16)
                state = decayed(state, b, row + 2 * p) + loc[b, at, :]
            send_ref[p * per : (p + 1) * per] = state.astype(BF16).reshape(per, po, LANES)

    contribute(8)
    chain(range(nb), 0, fpre, fsend)
    lax.fori_loop(1, nz, fcast_start, 0)
    frecv[z] = fsend[z]
    contribute(12)
    chain(range(nb - 1, -1, -1), 4, bpre, bsend)
    lax.fori_loop(1, nz, bcast_start, 0)
    brecv[z] = bsend[z]

    phase("p_gate")
    loads[8].wait()
    hids = (hid0, hid1, hid2)
    for t in (0, 2, 1):
        skip = nctx if t == 0 else 0
        rraw[8 + t * tile : 8 + (t + 1) * tile, :] = dot(hids[t][skip : skip + tile, :], wrd[...])
    for t in range(3):
        skip = nctx if t == 0 else 0
        gbuf[t * tile : (t + 1) * tile, :] = silu(dot(hids[t][skip : skip + tile, :], wog[...]))
    redge_up.wait_recv()
    redge_down.wait_recv()
    rraw[7:8, :] = redge[0, 7:8, :] * (1.0 - first)
    rraw[8 + span : 9 + span, :] = redge[1, 0:1, :] * (1.0 - last)

    def conv_reader(b, _):
        base = aligned(b, LANES)
        block = rraw[pl.ds(base, LANES + 16), :]
        rbf[pl.ds(base, LANES), :] = conv(block, slice(both, both + LANES)).astype(BF16)
        return 0

    lax.fori_loop(0, nb, conv_reader, 0)

    phase("p_inside")
    lower = lax.broadcasted_iota(jnp.int32, (LANES, LANES), 1) <= lax.broadcasted_iota(
        jnp.int32, (LANES, LANES), 0
    )
    upper = lax.broadcasted_iota(jnp.int32, (LANES, LANES), 1) >= lax.broadcasted_iota(
        jnp.int32, (LANES, LANES), 0
    )

    def inside(b, _):
        base = aligned(b, LANES)
        r = rbf[pl.ds(base, LANES), :]
        g = dot_nt(r, wbf[pl.ds(base, LANES), :])
        cl = xt[b]
        for p in range(npair):
            at = slice(p * LANES, (p + 1) * LANES)
            s = sbf[pl.ds(base, LANES), at]
            own = []
            for h in (2 * p, 2 * p + 1):
                arg = jnp.where(
                    lower,
                    cl[:, h : h + 1] - xrows[b, h : h + 1, :],
                    xrows[b, 4 + h : 5 + h, :] - cl[:, 4 + h : 5 + h],
                )
                wgt = jnp.where(lower, strow[b, h : h + 1, :], 0.0) + jnp.where(
                    upper, strow[b, 4 + h : 5 + h, :], 0.0
                )
                own.append(dot((g * jnp.exp(arg) * wgt).astype(BF16), s))
            carried = expand(cl, 16, p) * dot_nt(r, fpre[b, at, :]) + expand(cl, 20, p) * dot_nt(
                r, bpre[b, at, :]
            )
            ybuf[pl.ds(base, LANES), at] = carried + jnp.where(
                lane_iota((LANES, LANES)) < LANES // 2, own[0], own[1]
            )
        return 0

    def inside2(i, _):
        inside(2 * i, 0)
        inside(2 * i + 1, 0)
        return 0

    lax.fori_loop(0, nb // 2, inside2, 0)

    phase("p_fwait")

    def take_forward(d, _):
        src = lax.rem(z + nz - d, nz)
        remote(dsend, drecv.at[src], ds.at[d], dr.at[src], {"sp": src}).wait_recv()
        remote(ctsend.at[src], ctrecv.at[src], cs.at[d], cr.at[src], {"sp": src}).wait_recv()
        remote(fsend.at[src], frecv.at[src], fs.at[d], fr.at[src], {"sp": src}).wait_recv()
        return 0

    lax.fori_loop(1, nz, take_forward, 0)
    phase("p_fscan")
    for k in range(nz):
        dm[k : k + 1, :] = drecv[k]
    head = z * po // (LANES // 2)
    dall = dm[...]
    lane_z = lane_iota((nz, LANES))
    for i in range(4):
        col = jnp.sum(jnp.where(lane_z == 4 * i + head, dall, 0.0), axis=1, keepdims=True)
        ed[i] = jnp.exp(jnp.broadcast_to(col, (nz, LANES)))
    state = jnp.zeros((po, LANES), F32)
    for k in range(nz):
        state = ed[2, k : k + 1, :] * state + ctrecv[k, 0].astype(F32)
    for k in range(nz):
        fback[k] = state.astype(BF16)
        state = ed[0, k : k + 1, :] * state + frecv[k].astype(F32)

    def fret(d):
        t = lax.rem(z + d, nz)
        return remote(fback.at[t], fin.at[z], rs.at[d], rr.at[z], {"sp": t})

    def fret_start(d, _):
        fret(d).start()
        return 0

    def bret(d):
        t = lax.rem(z + d, nz)
        return remote(bback.at[t], bin_.at[z], rbs.at[d], rbr.at[z], {"sp": t})

    def bret_start(d, _):
        bret(d).start()
        return 0

    lax.fori_loop(1, nz, fret_start, 0)
    fin[z] = fback[z]
    phase("p_bwait")

    def take_backward(d, _):
        src = lax.rem(z + nz - d, nz)
        remote(bsend.at[src], brecv.at[src], bs.at[d], br.at[src], {"sp": src}).wait_recv()
        return 0

    lax.fori_loop(1, nz, take_backward, 0)
    phase("p_bscan")
    state = jnp.zeros((po, LANES), F32)
    for k in reversed(range(nz)):
        state = ed[3, k : k + 1, :] * state + ctrecv[k, 1].astype(F32)
    for k in reversed(range(nz)):
        bback[k] = state.astype(BF16)
        state = ed[1, k : k + 1, :] * state + brecv[k].astype(F32)
    lax.fori_loop(1, nz, bret_start, 0)
    bin_[z] = bback[z]
    phase("p_retwait")
    lat_copy.wait_send()
    for sent in (cedge_up, cedge_down, edge_up, edge_down, redge_up, redge_down):
        sent.wait_send()

    def drain_z(d, _):
        zcast(d).wait_send()
        ctcast(d).wait_send()
        gcast(d).wait_send()
        fcast(d).wait_send()
        bcast(d).wait_send()
        dcast(d).wait_send()
        return 0

    lax.fori_loop(1, nz, drain_z, 0)

    def drain_k(d, _):
        mcast(d).wait_send()
        return 0

    lax.fori_loop(1, nk, drain_k, 0)

    def take_return(d, _):
        src = lax.rem(z + nz - d, nz)
        remote(fback.at[src], fin.at[src], rs.at[d], rr.at[src], {"sp": src}).wait_recv()
        remote(bback.at[src], bin_.at[src], rbs.at[d], rbr.at[src], {"sp": src}).wait_recv()
        return 0

    def add_gate(d, total):
        src = lax.rem(z + nz - d, nz)
        remote(gpay, grecv.at[src], gzs.at[d], gzr.at[src], {"sp": src}).wait_recv()
        return total + grecv[src]

    gate = lax.fori_loop(1, nz, add_gate, gpay[...])
    lax.fori_loop(1, nz, take_return, 0)

    phase("p_finish")
    hrow = LANES // 2

    def piece(k, b):
        return nall.at[k, pl.ds(aligned(b, LANES), LANES)]

    def part(k, b, h):
        return nall.at[k, pl.ds(pl.multiple_of(b * LANES + h * hrow, hrow), hrow)]

    def to_partner(k, i, b):
        return remote(piece(k, b), piece(k, b), ps.at[i, b], pr.at[i, b], {"dp": 1 - c})

    k_left = left * 2 + c
    k_right = right * 2 + c
    k_far = lax.rem(x + 2, nx) * 2 + c

    def own_right(b):
        return remote(piece(me, b), piece(me, b), gs.at[0, b], gr.at[0, b], {"tp": right})

    def own_left(b):
        return remote(piece(me, b), piece(me, b), gs.at[1, b], gr.at[1, b], {"tp": left})

    def relay_right(b):
        return remote(part(k_left, b, 0), part(k_left, b, 0), gs2.at[0, b], gr2.at[0, b], {"tp": right})

    def relay_left(b):
        return remote(part(k_right, b, 1), part(k_right, b, 1), gs2.at[1, b], gr2.at[1, b], {"tp": left})

    def finish(b, _):
        base = aligned(b, LANES)
        r = rbf[pl.ds(base, LANES), :]
        cl = xt[b]
        vals = []
        for p in range(npair):
            at = slice(p * LANES, (p + 1) * LANES)
            per = LANES // po
            f_in = fin[p * per : (p + 1) * per].reshape(LANES, LANES)
            b_in = bin_[p * per : (p + 1) * per].reshape(LANES, LANES)
            yy = (
                ybuf[pl.ds(base, LANES), at]
                + expand(cl, 24, p) * dot_nt(r, f_in)
                + expand(cl, 28, p) * dot_nt(r, b_in)
            )
            vals.append(yy * gbuf[pl.ds(base, LANES), at])
        sq = sum(jnp.sum(a * a, axis=1, keepdims=True) for a in vals)
        inv = lax.rsqrt(sq / chan + EPSILON)
        for p in range(npair):
            at = slice(p * LANES, (p + 1) * LANES)
            nall[me, pl.ds(base, LANES), at] = (vals[p] * inv * ggain[:, at]).astype(BF16)
        own_right(b).start()
        own_left(b).start()
        to_partner(me, 0, b).start()
        return 0

    lax.fori_loop(0, nb, finish, 0)
    loads[9].wait()

    phase("p_collect")
    out0 = pl.multiple_of(me * cols, cols)

    flip = 1 - 2 * c

    def product(b, ks):
        base = aligned(b, LANES)
        total = None
        for k in ks:
            w = wout[pl.ds(aligned(k, chan), chan), :]
            part_sum = dot(nall[k, pl.ds(base, LANES), :], w)
            total = part_sum if total is None else total + part_sum
        return total

    def near(b):
        remote(piece(k_left, b), piece(k_left, b), gs.at[0, b], gr.at[0, b], {"tp": left}).wait_recv()
        relay_right(b).start()
        to_partner(k_left, 1, b).start()
        remote(piece(k_right, b), piece(k_right, b), gs.at[1, b], gr.at[1, b], {"tp": right}).wait_recv()
        relay_left(b).start()
        to_partner(k_right, 2, b).start()

    def near_product(b):
        for n, k in enumerate((me, k_left, k_right)):
            to_partner(k + flip, n, b).wait_recv()
        ks = (me, k_left, k_right, me + flip, k_left + flip, k_right + flip)
        oacc[pl.ds(aligned(b, LANES), LANES), :] = product(b, ks)

    near(0)

    def near_turn(b, _):
        near(b)
        near_product(b - 1)
        return 0

    lax.fori_loop(1, nb, near_turn, 0)
    near_product(nb - 1)
    phase("p_far")

    def far(b):
        for h in range(2):
            remote(part(k_far, b, h), part(k_far, b, h), gs2.at[h, b], gr2.at[h, b], {"tp": left}).wait_recv()
        to_partner(k_far, 3, b).start()

    def store(b):
        rows = pl.ds(aligned(b, LANES), LANES)
        return pltpu.make_async_copy(obuf.at[rows], out.at[rows], osem.at[b])

    def far_product(b):
        to_partner(k_far + flip, 3, b).wait_recv()
        rows = pl.ds(aligned(b, LANES), LANES)
        mix = oacc[rows, :] + product(b, (k_far, k_far + flip))
        res_rows = lat[rows, pl.ds(out0, cols)].astype(F32)
        obuf[rows, :] = (res_rows + gate * mix).astype(BF16)
        store(b).start()

    far(0)

    def far_turn(b, _):
        far(b)
        far_product(b - 1)
        return 0

    lax.fori_loop(1, nb, far_turn, 0)
    far_product(nb - 1)

    phase("p_drain")

    def drain_back(d, _):
        fret(d).wait_send()
        bret(d).wait_send()
        return 0

    lax.fori_loop(1, nz, drain_back, 0)

    def drain_b(b, _):
        own_right(b).wait_send()
        own_left(b).wait_send()
        relay_right(b).wait_send()
        relay_left(b).wait_send()
        for i in range(4):
            to_partner(me, i, b).wait_send()
        store(b).wait()
        return 0

    lax.fori_loop(0, nb, drain_b, 0)
    phase(None)


def on_device(
    latent,
    context,
    condition,
    context_condition,
    shift_weight,
    scale_weight,
    gate_weight,
    norm_gain,
    out_gate_weight,
    signal_weight,
    writer_weight,
    reader_matrix,
    step_weight,
    signal_taps,
    writer_taps,
    reader_taps,
    step_bias,
    decay_log,
    decay_extra,
    group_gain,
    output_weight,
):
    nz, nx = lax.axis_size("sp"), lax.axis_size("tp")
    half_rows, width = latent.shape
    span, nctx = 2 * half_rows, context.shape[0]
    chan, cols = out_gate_weight.shape[1], shift_weight.shape[1]
    nb, nk, po = span // LANES, 2 * nx, chan // nz
    full = chan + 2 * LANES
    tile = span // 3
    both = chan + LANES
    hbm = pl.BlockSpec(memory_space=pl.ANY)
    vmem = pl.BlockSpec(memory_space=pltpu.VMEM)
    dma = pltpu.SemaphoreType.DMA
    scratch = [
        ((8, width), F32),
        ((3, full), F32),
        ((3, *shift_weight.shape), BF16),
        ((span, width), BF16),
        ((nctx, width), BF16),
        ((nctx + tile, width), BF16),
        ((tile, width), BF16),
        ((tile, width), BF16),
        ((nctx + tile, full), F32),
        ((width, chan), BF16),
        ((width, chan), BF16),
        ((width, 2 * LANES), BF16),
        ((width, LANES), BF16),
        (output_weight.shape, BF16),
        ((cols // LANES * 4, LANES), BF16),
        ((nz, cols // LANES * 4, LANES), BF16),
        ((1, cols), F32),
        ((nz, 1, cols), F32),
        ((cols // LANES * 4, LANES), F32),
        ((nk, cols // LANES * 4, LANES), F32),
        ((8, width), F32),
        ((span, LANES), F32),
        ((nctx, LANES), F32),
        ((nctx + 16, both), F32),
        ((2, 8, both), F32),
        ((LANES, LANES), F32),
        ((span + 16, both), F32),
        ((2, 8, both), F32),
        ((span + 16, LANES), F32),
        ((2, 8, LANES), F32),
        ((2, 8, LANES), F32),
        ((span, chan), F32),
        ((span, LANES), F32),
        ((span, chan), BF16),
        ((span, LANES), BF16),
        ((span, LANES), BF16),
        ((nb, 8, LANES), F32),
        ((nb, 8, LANES), F32),
        ((-(-nb // 4) * 4, 32, LANES), F32),
        ((nb, LANES, 32), F32),
        ((nb, 8, LANES), F32),
        ((nb, chan, LANES), F32),
        ((nb, chan, LANES), BF16),
        ((nb, chan, LANES), BF16),
        ((nz, po, LANES), BF16),
        ((nz, po, LANES), BF16),
        ((nz, po, LANES), BF16),
        ((nz, po, LANES), BF16),
        ((nz, 2, po, LANES), BF16),
        ((nz, 2, po, LANES), BF16),
        ((1, LANES), F32),
        ((nz, 1, LANES), F32),
        ((nz, LANES), F32),
        ((4, nz, LANES), F32),
        ((nz, po, LANES), BF16),
        ((nz, po, LANES), BF16),
        ((nz, po, LANES), BF16),
        ((nz, po, LANES), BF16),
        ((span, chan), F32),
        ((nk, span, chan), BF16),
        ((span, cols), F32),
        ((span, cols), BF16),
    ]
    sems = (
        [(10,), (nz,), (nz,), (nk,), (nk,)]
        + [(2,)] * 6
        + [(nz,)] * 14
        + [None, None]
        + [(2, nb)] * 4
        + [(4, nb)] * 2
        + [(nb,)]
    )
    return pl.pallas_call(
        functools.partial(kernel, nz, nx),
        out_shape=jax.ShapeDtypeStruct((span, cols), BF16),
        in_specs=[hbm] * 10 + [vmem] * 11,
        out_specs=hbm,
        scratch_shapes=[pltpu.VMEM(s, t) for s, t in scratch]
        + [dma if s is None else dma(s) for s in sems],
        compiler_params=pltpu.CompilerParams(
            collective_id=0, has_side_effects=True, vmem_limit_bytes=56 * 1024 * 1024
        ),
        name="mixing",
    )(
        latent,
        context,
        shift_weight,
        scale_weight,
        gate_weight,
        out_gate_weight,
        signal_weight,
        writer_weight,
        reader_matrix,
        output_weight,
        condition,
        context_condition,
        jnp.transpose(step_weight, (0, 2, 1)),
        norm_gain.reshape(1, width),
        signal_taps,
        writer_taps,
        reader_taps,
        step_bias,
        decay_log,
        decay_extra,
        group_gain.reshape(1, chan),
    )


def solution(mesh):
    in_specs = (
        P(("grp", "sp", "dp"), None),
        P(("grp", "sp"), None),
        P("grp"),
        P(),
        P("sp", ("tp", "dp")),
        P("sp", ("tp", "dp")),
        P("sp", ("tp", "dp")),
        P(),
        P(None, ("tp", "dp")),
        P(None, ("tp", "dp")),
        P(None, ("tp", "dp")),
        P(None, ("tp", "dp")),
        P(None, None, ("tp", "dp")),
        P(None, ("tp", "dp")),
        P(None, ("tp", "dp")),
        P(None, ("tp", "dp")),
        P(None, ("tp", "dp")),
        P(None, ("tp", "dp")),
        P(None, ("tp", "dp"), ("grp", "sp")),
        P(("tp", "dp")),
        P(None, ("tp", "dp")),
    )
    out_specs = P(("grp", "sp"), ("tp", "dp"))
    return jax.shard_map(
        on_device, mesh=mesh, in_specs=in_specs, out_specs=out_specs, check_vma=False
    )
```

time: 116 us -> 96.8 us (0.83)
  Pallas kernels: 105 us -> 94.5 us
  local copies, waits for them, and re-layouts: 9.07 us -> 2.06 us
  other arithmetic: 2.02 us -> 0 us
    pallas_call x1, Pallas kernels: 105 us -> 94.5 us  [on_device(): pl.pallas_call(functools.partial(kernel, nz, nx), out_shape=jax.ShapeDtyp...]
    reshape x4 -> x0, local copies, waits for them, and re-layouts: 5.51 us -> none  [the longest x1 1.47 us: on_device(): stepw = jnp.transpose(step_weight, (0, 2, 1)).reshape(rows8, width)]
    concatenate x2 -> x0, other arithmetic: 2.02 us -> none  [the longest x1 1.32 us: on_device(): taps = jnp.concatenate([signal_taps, writer_taps, reader_taps], axis=1)]
    broadcast_in_dim x3 -> x0, local copies, waits for them, and re-layouts: 1.42 us -> none  [the longest x1 0.71 us: on_device(): context_condition[None]]
where the time goes in v2:
time: 96.8 us; the launch traced here: 96.6 us
  Pallas kernels  94.5 us (98%)
  local copies, waits for them, and re-layouts  2.06 us (2%)
    pallas_call x1, Pallas kernels, on_device(): pl.pallas_call(functools.partial(kernel, nz, nx), out_shape=jax.ShapeDtyp...  94.5 us
    unnamed x1, local copies, waits for them, and re-layouts  2.06 us

profile of v2, /device:TPU:33, one launch (start us, length us, event | category | flops | bytes accessed | tf_op | source)
XLA Modules:
  0.0 96.6 jit_solution(10645417698417791413)
XLA Ops:
  0.0 94.5 %mixing.1 = bf16[768,512]{1,0:T(8,128)(2,1)} custom-call(bf16[384,4096]{1,0:T(8,128)(2,1)} %latent.1, bf16[32,4096]{1,0:T(8,128)(2,1)} %context.1, bf16[256,512]{1,0:T(8,128)(2,1)} %shift_w.1, bf16[256,512]{1,0:T(8,128)(2,1)} %scale_w.1, bf16[256,512]{1,0:T(8,128)(2,1)} %gate_w.1, bf16[4096,256]{1,0:T(8,128)(2,1)} %og_w.1, bf16[4096,256]{1,0:T(8,128)(2,1)} %sg_w.1, ...), custom_call_target="tpu_custom_call" | custom-call | tf_op jit(solution)/shard_map/mixing/pallas_call | solution.py:1048
  94.5 2.1 %copy.23 = bf16[768,512]{1,0:T(8,128)(2,1)} copy(bf16[768,512]{1,0:T(8,128)(2,1)} %mixing.1) | data formatting | bytes 1572864

commit v3 on v2

--- a/solution.py
+++ b/solution.py
@@ -74,115 +74,132 @@
     wr_w,
     rd_w,
     out_w,
-    cond,
-    ctx_cond,
-    stepw_in,
-    gain,
-    signal_taps,
-    writer_taps,
-    reader_taps,
-    bias_in,
-    dlog_in,
-    extra,
-    ggain,
-    out,
-    condrow,
-    taps,
-    mw,
-    lat,
-    ctx,
-    hid0,
-    hid1,
-    hid2,
-    acc,
-    wog,
-    wsg,
-    wsw,
-    wrd,
-    wout,
-    pay,
-    zrecv,
-    gpay,
-    grecv,
-    msum,
-    mods,
-    ab,
-    rinv,
-    rinvc,
-    craw,
-    cedge,
-    cstepc,
-    raw,
-    edge,
-    rraw,
-    redge,
-    rsend,
-    gbuf,
-    stepc,
-    sbf,
-    wbf,
-    rbf,
-    ldrow,
-    strow,
-    xrows,
-    xt,
-    eexp,
-    loc,
-    fpre,
-    bpre,
-    fsend,
-    frecv,
-    bsend,
-    brecv,
-    ctsend,
-    ctrecv,
-    dsend,
-    drecv,
-    dm,
-    ed,
-    fback,
-    fin,
-    bback,
-    bin_,
-    ybuf,
-    nall,
-    oacc,
-    obuf,
-    lsem,
-    zs,
-    zr,
-    ms,
-    mr,
-    es,
-    er,
-    res,
-    rer,
-    ces,
-    cer,
-    gzs,
-    gzr,
-    fs,
-    fr,
-    bs,
-    br,
-    cs,
-    cr,
-    ds,
-    dr,
-    rs,
-    rr,
-    rbs,
-    rbr,
-    lats,
-    latr,
-    gs,
-    gr,
-    gs2,
-    gr2,
-    ps,
-    pr,
-    osem,
+    *rest,
 ):
+    small_in, rest = rest[:11], rest[11:]
+    (
+        out,
+        cond,
+        ctx_cond,
+        stepw_in,
+        gain,
+        signal_taps,
+        writer_taps,
+        reader_taps,
+        bias_in,
+        dlog_in,
+        extra,
+        ggain,
+        condrow,
+        taps,
+        mw,
+        lat,
+        ctx,
+        hid0,
+        hid1,
+        hid2,
+        acc,
+        wog,
+        wsg,
+        wsw,
+        wrd,
+        wout,
+        pay,
+        zrecv,
+        gpay,
+        grecv,
+        msum,
+        mods,
+        ab,
+        rinv,
+        rinvc,
+        craw,
+        cedge,
+        cstepc,
+        raw,
+        edge,
+        rraw,
+        redge,
+        rsend,
+        gbuf,
+        stepc,
+        sbf,
+        wtr,
+        rbf,
+        ldrow,
+        strow,
+        xrows,
+        xt,
+        eexp,
+        loc,
+        fpre,
+        bpre,
+        fsend,
+        frecv,
+        bsend,
+        brecv,
+        ctsend,
+        ctrecv,
+        dsend,
+        drecv,
+        dm,
+        ed,
+        fback,
+        fin,
+        bback,
+        bin_,
+        ybuf,
+        nall,
+        oacc,
+        obuf,
+        lsem,
+        zs,
+        zr,
+        ms,
+        mr,
+        es,
+        er,
+        res,
+        rer,
+        ces,
+        cer,
+        gzs,
+        gzr,
+        fs,
+        fr,
+        bs,
+        br,
+        cs,
+        cr,
+        ds,
+        dr,
+        rs,
+        rr,
+        rbs,
+        rbr,
+        lats,
+        latr,
+        gs,
+        gr,
+        gs2,
+        gr2,
+        ps,
+        pr,
+        osem,
+    ) = rest
+    small = (
+        cond,
+        ctx_cond,
+        stepw_in,
+        gain,
+        signal_taps,
+        writer_taps,
+        reader_taps,
+        bias_in,
+        dlog_in,
+        extra,
+        ggain,
+    )
     scopes = []
 
     def phase(name):
@@ -223,11 +240,9 @@
         (rd_w, wrd),
         (og_w, wog),
         (out_w, wout),
+        *zip(small_in, small),
     ]
     loads = [pltpu.make_async_copy(s, d, lsem.at[i]) for i, (s, d) in enumerate(pairs)]
-    for load in loads:
-        load.start()
-
     barrier = pltpu.get_barrier_semaphore()
 
     def greet_z(d, _):
@@ -243,10 +258,14 @@
 
     lax.fori_loop(1, nz, greet_z, 0)
     lax.fori_loop(1, nk, greet_k, 0)
+    for i in (10, 11, *range(10), *range(12, len(loads))):
+        loads[i].start()
 
     phase("p_matvec")
     zrows = shift_w.shape[0]
     condrow[...] = jnp.zeros_like(condrow)
+    loads[10].wait()
+    loads[11].wait()
     condrow[0:1, :] = cond[...].astype(F32).reshape(1, width)
     condrow[1:2, :] = ctx_cond[...].astype(F32).reshape(1, width)
     act = silu(condrow[:, pl.ds(aligned(z, zrows), zrows)]).astype(BF16)
@@ -272,6 +291,9 @@
     lax.fori_loop(1, nz, zcast_start, 0)
     lat_copy = remote(latent, lat.at[pl.ds(own0, half_rows)], lats, latr, {"dp": 1 - c})
     lat_copy.start()
+
+    for i in range(12, len(loads)):
+        loads[i].wait()
 
     taps[:, 0:chan] = signal_taps[...]
     taps[:, chan : chan + LANES] = writer_taps[...]
@@ -408,48 +430,31 @@
 
             lax.fori_loop(0, steps, turn, 0)
 
-    def mod_first(kk, _):
+    def mod_ctx(kk, _):
         modulate(ctx, 0, nctx, rinvc, 2, hid0, 0, kk)
-        modulate(lat, 0, tile, rinv, 0, hid0, nctx, kk)
-        return 0
-
-    lax.fori_loop(0, steps, mod_first, 0)
+        return 0
+
+    lax.fori_loop(0, steps, mod_ctx, 0)
     for i in range(5, 7):
         loads[i].wait()
-    phase("p_dots0")
-    multiply(hid0)
-    modulate_tile(2, hid2)
+    multiply(hid0.at[0:nctx])
     craw[8 : 8 + nctx, :] = acc[0:nctx, 0:both]
     cstepc[0:nctx, :] = acc[0:nctx, both : both + LANES]
-    raw[8 : 8 + tile, :] = acc[nctx : nctx + tile, 0:both]
-    stepc[0:tile, :] = acc[nctx : nctx + tile, both : both + LANES]
     cedge_up = remote(craw.at[nctx : nctx + 8], cedge.at[0], ces.at[0], cer.at[0], {"sp": up})
     cedge_down = remote(craw.at[8:16], cedge.at[1], ces.at[1], cer.at[1], {"sp": down})
     cedge_up.start()
     cedge_down.start()
-    phase("p_dots2")
-    multiply(hid2)
-    modulate_tile(1, hid1)
-    raw[8 + 2 * tile : 8 + 3 * tile, :] = acc[0:tile, 0:both]
-    stepc[2 * tile : 3 * tile, :] = acc[0:tile, both : both + LANES]
-    edge_up = remote(raw.at[span : span + 8], edge.at[0], es.at[0], er.at[0], {"sp": up})
-    edge_down = remote(raw.at[8:16], edge.at[1], es.at[1], er.at[1], {"sp": down})
-    edge_up.start()
-    edge_down.start()
-    loads[7].wait()
-    ends = jnp.concatenate([hid0[nctx : nctx + 16, :], hid2[tile - 16 : tile, :]], axis=0)
-    rends = dot(ends, wrd[...])
-    rsend[0] = rends[24:32, :]
-    rsend[1] = rends[0:8, :]
-    redge_up = remote(rsend.at[0], redge.at[0], res.at[0], rer.at[0], {"sp": up})
-    redge_down = remote(rsend.at[1], redge.at[1], res.at[1], rer.at[1], {"sp": down})
-    redge_up.start()
-    redge_down.start()
-    phase("p_dots1")
-    multiply(hid1)
-    raw[8 + tile : 8 + 2 * tile, :] = acc[0:tile, 0:both]
-    stepc[tile : 2 * tile, :] = acc[0:tile, both : both + LANES]
-
+
+    def mod_first(kk, _):
+        modulate(lat, 0, tile, rinv, 0, hid0, nctx, kk)
+        return 0
+
+    lax.fori_loop(0, steps, mod_first, 0)
+    phase("p_dots0")
+    modulate_tile(2, hid2)
+    multiply(hid0.at[nctx : nctx + tile])
+    raw[8 : 8 + tile, :] = acc[0:tile, 0:both]
+    stepc[0:tile, :] = acc[0:tile, both : both + LANES]
     phase("p_ctxstate")
     def conv(block, at):
         n = block.shape[0]
@@ -507,6 +512,30 @@
 
     lax.fori_loop(1, nz, ctcast_start, 0)
     ctrecv[z] = ctsend[z]
+    phase("p_dots2")
+    modulate_tile(1, hid1)
+    multiply(hid2)
+    raw[8 + 2 * tile : 8 + 3 * tile, :] = acc[0:tile, 0:both]
+    stepc[2 * tile : 3 * tile, :] = acc[0:tile, both : both + LANES]
+    edge_up = remote(raw.at[span : span + 8], edge.at[0], es.at[0], er.at[0], {"sp": up})
+    edge_down = remote(raw.at[8:16], edge.at[1], es.at[1], er.at[1], {"sp": down})
+    edge_up.start()
+    edge_down.start()
+    loads[7].wait()
+    ends = jnp.concatenate([hid0[nctx : nctx + 16, :], hid2[tile - 16 : tile, :]], axis=0)
+    rends = dot(ends, wrd[...])
+    rsend[0] = rends[24:32, :]
+    rsend[1] = rends[0:8, :]
+    redge_up = remote(rsend.at[0], redge.at[0], res.at[0], rer.at[0], {"sp": up})
+    redge_down = remote(rsend.at[1], redge.at[1], res.at[1], rer.at[1], {"sp": down})
+    redge_up.start()
+    redge_down.start()
+
+    phase("p_dots1")
+    multiply(hid1)
+    raw[8 + tile : 8 + 2 * tile, :] = acc[0:tile, 0:both]
+    stepc[tile : 2 * tile, :] = acc[0:tile, both : both + LANES]
+
     phase("p_edge")
     edge_up.wait_recv()
     edge_down.wait_recv()
@@ -519,11 +548,11 @@
         base = aligned(b, LANES)
         for j in range(chan // LANES + 1):
             at = slice(j * LANES, (j + 1) * LANES)
-            val = conv(raw[pl.ds(base, LANES + 16), at], at).astype(BF16)
+            val = conv(raw[pl.ds(base, LANES + 16), at], at)
             if j < chan // LANES:
-                sbf[pl.ds(base, LANES), at] = val
+                sbf[pl.ds(base, LANES), at] = val.astype(BF16)
             else:
-                wbf[pl.ds(base, LANES), :] = val
+                wtr[b] = jnp.transpose(val).astype(BF16)
         return 0
 
     lax.fori_loop(0, nb, conv_block, 0)
@@ -564,10 +593,12 @@
 
     phase("p_states")
     npair = chan // LANES
-    def decayed(state, b, row):
-        lo = eexp[b, row : row + 1, :]
-        hi = eexp[b, row + 1 : row + 2, :]
-        return jnp.where(row_iota((LANES, LANES)) < LANES // 2, lo, hi) * state
+    def decays(b, row):
+        lanes = lane_iota((1, LANES)) < LANES // 2
+        return [
+            jnp.where(lanes, eexp[b, r : r + 1, :], eexp[b, r + 1 : r + 2, :])
+            for r in range(row, row + 2 * npair, 2)
+        ]
 
     sub8 = row_iota((8, LANES))
     dsend[...] = jnp.sum(
@@ -604,23 +635,26 @@
 
     def contribute(first):
         for b in range(nb):
-            base = b * LANES
-            w = wbf[base : base + LANES, :]
             cl = xt[b]
+            parts = [
+                sbf[b * LANES : (b + 1) * LANES, p * LANES : (p + 1) * LANES].astype(F32)
+                * expand(cl, first, p)
+                for p in range(npair)
+            ]
+            loc[b] = dot(wtr[b], jnp.concatenate(parts, axis=1).astype(BF16))
+
+    def chain(order, row, before_ref, send_ref):
+        per = LANES // po
+        state = [jnp.zeros((LANES, LANES), F32) for _ in range(npair)]
+        for b in order:
+            by = decays(b, row)
             for p in range(npair):
                 at = slice(p * LANES, (p + 1) * LANES)
-                v = sbf[base : base + LANES, at].astype(F32) * expand(cl, first, p)
-                loc[b, at, :] = dot_tn(v.astype(BF16), w)
-
-    def chain(order, row, before_ref, send_ref):
-        per = LANES // po
+                before_ref[b, :, at] = state[p].astype(BF16)
+                state[p] = state[p] * by[p] + loc[b, :, at]
         for p in range(npair):
-            at = slice(p * LANES, (p + 1) * LANES)
-            state = jnp.zeros((LANES, LANES), F32)
-            for b in order:
-                before_ref[b, at, :] = state.astype(BF16)
-                state = decayed(state, b, row + 2 * p) + loc[b, at, :]
-            send_ref[p * per : (p + 1) * per] = state.astype(BF16).reshape(per, po, LANES)
+            turned = jnp.transpose(state[p]).astype(BF16)
+            send_ref[p * per : (p + 1) * per] = turned.reshape(per, po, LANES)
 
     contribute(8)
     chain(range(nb), 0, fpre, fsend)
@@ -664,7 +698,9 @@
     def inside(b, _):
         base = aligned(b, LANES)
         r = rbf[pl.ds(base, LANES), :]
-        g = dot_nt(r, wbf[pl.ds(base, LANES), :])
+        g = dot(r, wtr[b])
+        from_left = dot(r, fpre[b])
+        from_right = dot(r, bpre[b])
         cl = xt[b]
         for p in range(npair):
             at = slice(p * LANES, (p + 1) * LANES)
@@ -680,9 +716,7 @@
                     upper, strow[b, 4 + h : 5 + h, :], 0.0
                 )
                 own.append(dot((g * jnp.exp(arg) * wgt).astype(BF16), s))
-            carried = expand(cl, 16, p) * dot_nt(r, fpre[b, at, :]) + expand(cl, 20, p) * dot_nt(
-                r, bpre[b, at, :]
-            )
+            carried = expand(cl, 16, p) * from_left[:, at] + expand(cl, 20, p) * from_right[:, at]
             ybuf[pl.ds(base, LANES), at] = carried + jnp.where(
                 lane_iota((LANES, LANES)) < LANES // 2, own[0], own[1]
             )
@@ -970,9 +1004,20 @@
     tile = span // 3
     both = chan + LANES
     hbm = pl.BlockSpec(memory_space=pl.ANY)
-    vmem = pl.BlockSpec(memory_space=pltpu.VMEM)
     dma = pltpu.SemaphoreType.DMA
+    heads = step_bias.shape[1]
     scratch = [
+        (condition.shape, BF16),
+        (context_condition.shape, BF16),
+        ((2, heads, width), BF16),
+        ((1, width), F32),
+        (signal_taps.shape, F32),
+        (writer_taps.shape, F32),
+        (reader_taps.shape, F32),
+        (step_bias.shape, F32),
+        (decay_log.shape, F32),
+        (decay_extra.shape, F32),
+        ((1, chan), F32),
         ((8, width), F32),
         ((3, full), F32),
         ((3, *shift_weight.shape), BF16),
@@ -1007,16 +1052,16 @@
         ((span, chan), F32),
         ((span, LANES), F32),
         ((span, chan), BF16),
-        ((span, LANES), BF16),
+        ((nb, LANES, LANES), BF16),
         ((span, LANES), BF16),
         ((nb, 8, LANES), F32),
         ((nb, 8, LANES), F32),
         ((-(-nb // 4) * 4, 32, LANES), F32),
         ((nb, LANES, 32), F32),
         ((nb, 8, LANES), F32),
-        ((nb, chan, LANES), F32),
-        ((nb, chan, LANES), BF16),
-        ((nb, chan, LANES), BF16),
+        ((nb, LANES, chan), F32),
+        ((nb, LANES, chan), BF16),
+        ((nb, LANES, chan), BF16),
         ((nz, po, LANES), BF16),
         ((nz, po, LANES), BF16),
         ((nz, po, LANES), BF16),
@@ -1037,7 +1082,7 @@
         ((span, cols), BF16),
     ]
     sems = (
-        [(10,), (nz,), (nz,), (nk,), (nk,)]
+        [(21,), (nz,), (nz,), (nk,), (nk,)]
         + [(2,)] * 6
         + [(nz,)] * 14
         + [None, None]
@@ -1048,7 +1093,7 @@
     return pl.pallas_call(
         functools.partial(kernel, nz, nx),
         out_shape=jax.ShapeDtypeStruct((span, cols), BF16),
-        in_specs=[hbm] * 10 + [vmem] * 11,
+        in_specs=[hbm] * 21,
         out_specs=hbm,
         scratch_shapes=[pltpu.VMEM(s, t) for s, t in scratch]
         + [dma if s is None else dma(s) for s in sems],

time: 96.8 us -> 96.5 us (level)
  no operation moved by 1% of the time
where the time goes in v3:
time: 96.5 us; the launch traced here: 96.4 us
  Pallas kernels  94.3 us (98%)
  local copies, waits for them, and re-layouts  2.06 us (2%)
    pallas_call x1, Pallas kernels, on_device(): pl.pallas_call(functools.partial(kernel, nz, nx), out_shape=jax.ShapeDtyp...  94.3 us
    unnamed x1, local copies, waits for them, and re-layouts  2.06 us

profile of v3, /device:TPU:33, one launch (start us, length us, event | category | flops | bytes accessed | tf_op | source)
XLA Modules:
  0.0 96.4 jit_solution(16779110059332070649)
XLA Ops:
  0.0 94.3 %mixing.1 = bf16[768,512]{1,0:T(8,128)(2,1)} custom-call(bf16[384,4096]{1,0:T(8,128)(2,1)} %latent.1, bf16[32,4096]{1,0:T(8,128)(2,1)} %context.1, bf16[256,512]{1,0:T(8,128)(2,1)} %shift_w.1, bf16[256,512]{1,0:T(8,128)(2,1)} %scale_w.1, bf16[256,512]{1,0:T(8,128)(2,1)} %gate_w.1, bf16[4096,256]{1,0:T(8,128)(2,1)} %og_w.1, bf16[4096,256]{1,0:T(8,128)(2,1)} %sg_w.1, ...), custom_call_target="tpu_custom_call" | custom-call | tf_op jit(solution)/shard_map/mixing/pallas_call | solution.py:1093
  94.3 2.1 %copy.23 = bf16[768,512]{1,0:T(8,128)(2,1)} copy(bf16[768,512]{1,0:T(8,128)(2,1)} %mixing.1) | data formatting | bytes 1572864

commit v4 on v3

--- a/solution.py
+++ b/solution.py
@@ -95,6 +95,7 @@
         mw,
         lat,
         ctx,
+        hidc,
         hid0,
         hid1,
         hid2,
@@ -121,6 +122,7 @@
         rraw,
         redge,
         rsend,
+        esend,
         gbuf,
         stepc,
         sbf,
@@ -431,28 +433,41 @@
             lax.fori_loop(0, steps, turn, 0)
 
     def mod_ctx(kk, _):
-        modulate(ctx, 0, nctx, rinvc, 2, hid0, 0, kk)
+        modulate(ctx, 0, nctx, rinvc, 2, hidc, 0, kk)
+        modulate(lat, 0, 32, rinv, 0, hidc, nctx, kk)
+        modulate(lat, span - 32, 32, rinv, 0, hidc, nctx + 32, kk)
         return 0
 
     lax.fori_loop(0, steps, mod_ctx, 0)
-    for i in range(5, 7):
+    for i in range(5, 8):
         loads[i].wait()
-    multiply(hid0.at[0:nctx])
+    multiply(hidc)
     craw[8 : 8 + nctx, :] = acc[0:nctx, 0:both]
     cstepc[0:nctx, :] = acc[0:nctx, both : both + LANES]
     cedge_up = remote(craw.at[nctx : nctx + 8], cedge.at[0], ces.at[0], cer.at[0], {"sp": up})
     cedge_down = remote(craw.at[8:16], cedge.at[1], ces.at[1], cer.at[1], {"sp": down})
     cedge_up.start()
     cedge_down.start()
+    esend[0] = acc[nctx + 56 : nctx + 64, 0:both]
+    esend[1] = acc[nctx : nctx + 8, 0:both]
+    rends = dot(hidc[nctx : nctx + 64, :], wrd[...])
+    rsend[0] = rends[56:64, :]
+    rsend[1] = rends[0:8, :]
+    edge_up = remote(esend.at[0], edge.at[0], es.at[0], er.at[0], {"sp": up})
+    edge_down = remote(esend.at[1], edge.at[1], es.at[1], er.at[1], {"sp": down})
+    redge_up = remote(rsend.at[0], redge.at[0], res.at[0], rer.at[0], {"sp": up})
+    redge_down = remote(rsend.at[1], redge.at[1], res.at[1], rer.at[1], {"sp": down})
+    for sent in (edge_up, edge_down, redge_up, redge_down):
+        sent.start()
 
     def mod_first(kk, _):
-        modulate(lat, 0, tile, rinv, 0, hid0, nctx, kk)
+        modulate(lat, 0, tile, rinv, 0, hid0, 0, kk)
         return 0
 
     lax.fori_loop(0, steps, mod_first, 0)
     phase("p_dots0")
     modulate_tile(2, hid2)
-    multiply(hid0.at[nctx : nctx + tile])
+    multiply(hid0)
     raw[8 : 8 + tile, :] = acc[0:tile, 0:both]
     stepc[0:tile, :] = acc[0:tile, both : both + LANES]
     phase("p_ctxstate")
@@ -517,20 +532,6 @@
     multiply(hid2)
     raw[8 + 2 * tile : 8 + 3 * tile, :] = acc[0:tile, 0:both]
     stepc[2 * tile : 3 * tile, :] = acc[0:tile, both : both + LANES]
-    edge_up = remote(raw.at[span : span + 8], edge.at[0], es.at[0], er.at[0], {"sp": up})
-    edge_down = remote(raw.at[8:16], edge.at[1], es.at[1], er.at[1], {"sp": down})
-    edge_up.start()
-    edge_down.start()
-    loads[7].wait()
-    ends = jnp.concatenate([hid0[nctx : nctx + 16, :], hid2[tile - 16 : tile, :]], axis=0)
-    rends = dot(ends, wrd[...])
-    rsend[0] = rends[24:32, :]
-    rsend[1] = rends[0:8, :]
-    redge_up = remote(rsend.at[0], redge.at[0], res.at[0], rer.at[0], {"sp": up})
-    redge_down = remote(rsend.at[1], redge.at[1], res.at[1], rer.at[1], {"sp": down})
-    redge_up.start()
-    redge_down.start()
-
     phase("p_dots1")
     multiply(hid1)
     raw[8 + tile : 8 + 2 * tile, :] = acc[0:tile, 0:both]
@@ -669,11 +670,9 @@
     loads[8].wait()
     hids = (hid0, hid1, hid2)
     for t in (0, 2, 1):
-        skip = nctx if t == 0 else 0
-        rraw[8 + t * tile : 8 + (t + 1) * tile, :] = dot(hids[t][skip : skip + tile, :], wrd[...])
+        rraw[8 + t * tile : 8 + (t + 1) * tile, :] = dot(hids[t][...], wrd[...])
     for t in range(3):
-        skip = nctx if t == 0 else 0
-        gbuf[t * tile : (t + 1) * tile, :] = silu(dot(hids[t][skip : skip + tile, :], wog[...]))
+        gbuf[t * tile : (t + 1) * tile, :] = silu(dot(hids[t][...], wog[...]))
     redge_up.wait_recv()
     redge_down.wait_recv()
     rraw[7:8, :] = redge[0, 7:8, :] * (1.0 - first)
@@ -1023,10 +1022,11 @@
         ((3, *shift_weight.shape), BF16),
         ((span, width), BF16),
         ((nctx, width), BF16),
-        ((nctx + tile, width), BF16),
+        ((nctx + 64, width), BF16),
         ((tile, width), BF16),
         ((tile, width), BF16),
-        ((nctx + tile, full), F32),
+        ((tile, width), BF16),
+        ((tile, full), F32),
         ((width, chan), BF16),
         ((width, chan), BF16),
         ((width, 2 * LANES), BF16),
@@ -1049,6 +1049,7 @@
         ((span + 16, LANES), F32),
         ((2, 8, LANES), F32),
         ((2, 8, LANES), F32),
+        ((2, 8, both), F32),
         ((span, chan), F32),
         ((span, LANES), F32),
         ((span, chan), BF16),

time: 96.5 us -> 93.5 us (0.969)
  Pallas kernels: 94.3 us -> 91.3 us
    pallas_call x1, Pallas kernels: 94.3 us -> 91.3 us  [on_device(): pl.pallas_call(functools.partial(kernel, nz, nx), out_shape=jax.ShapeDtyp...]
where the time goes in v4:
time: 93.5 us; the launch traced here: 93.3 us
  Pallas kernels  91.3 us (98%)
  local copies, waits for them, and re-layouts  2.06 us (2%)
    pallas_call x1, Pallas kernels, on_device(): pl.pallas_call(functools.partial(kernel, nz, nx), out_shape=jax.ShapeDtyp...  91.3 us
    unnamed x1, local copies, waits for them, and re-layouts  2.06 us

profile of v4, /device:TPU:33, one launch (start us, length us, event | category | flops | bytes accessed | tf_op | source)
XLA Modules:
  0.0 93.3 jit_solution(17274949992296586474)
XLA Ops:
  0.0 91.3 %mixing.1 = bf16[768,512]{1,0:T(8,128)(2,1)} custom-call(bf16[384,4096]{1,0:T(8,128)(2,1)} %latent.1, bf16[32,4096]{1,0:T(8,128)(2,1)} %context.1, bf16[256,512]{1,0:T(8,128)(2,1)} %shift_w.1, bf16[256,512]{1,0:T(8,128)(2,1)} %scale_w.1, bf16[256,512]{1,0:T(8,128)(2,1)} %gate_w.1, bf16[4096,256]{1,0:T(8,128)(2,1)} %og_w.1, bf16[4096,256]{1,0:T(8,128)(2,1)} %sg_w.1, ...), custom_call_target="tpu_custom_call" | custom-call | tf_op jit(solution)/shard_map/mixing/pallas_call | solution.py:1094
  91.3 2.1 %copy.23 = bf16[768,512]{1,0:T(8,128)(2,1)} copy(bf16[768,512]{1,0:T(8,128)(2,1)} %mixing.1) | data formatting | bytes 1572864

commit v5 on v4

--- a/solution.py
+++ b/solution.py
@@ -813,7 +813,6 @@
 
     def take_return(d, _):
         src = lax.rem(z + nz - d, nz)
-        remote(fback.at[src], fin.at[src], rs.at[d], rr.at[src], {"sp": src}).wait_recv()
         remote(bback.at[src], bin_.at[src], rbs.at[d], rbr.at[src], {"sp": src}).wait_recv()
         return 0
 
@@ -823,6 +822,26 @@
         return total + grecv[src]
 
     gate = lax.fori_loop(1, nz, add_gate, gpay[...])
+
+    def take_left(d, _):
+        src = lax.rem(z + nz - d, nz)
+        remote(fback.at[src], fin.at[src], rs.at[d], rr.at[src], {"sp": src}).wait_recv()
+        return 0
+
+    lax.fori_loop(1, nz, take_left, 0)
+
+    def add_left(b, _):
+        rows = pl.ds(aligned(b, LANES), LANES)
+        r = rbf[rows, :]
+        cl = xt[b]
+        per = LANES // po
+        for p in range(npair):
+            at = slice(p * LANES, (p + 1) * LANES)
+            f_in = fin[p * per : (p + 1) * per].reshape(LANES, LANES)
+            ybuf[rows, at] += expand(cl, 24, p) * dot_nt(r, f_in)
+        return 0
+
+    lax.fori_loop(0, nb, add_left, 0)
     lax.fori_loop(1, nz, take_return, 0)
 
     phase("p_finish")
@@ -861,11 +880,9 @@
         for p in range(npair):
             at = slice(p * LANES, (p + 1) * LANES)
             per = LANES // po
-            f_in = fin[p * per : (p + 1) * per].reshape(LANES, LANES)
             b_in = bin_[p * per : (p + 1) * per].reshape(LANES, LANES)
             yy = (
                 ybuf[pl.ds(base, LANES), at]
-                + expand(cl, 24, p) * dot_nt(r, f_in)
                 + expand(cl, 28, p) * dot_nt(r, b_in)
             )
             vals.append(yy * gbuf[pl.ds(base, LANES), at])

time: 93.5 us -> 93.4 us (level)
  no operation moved by 1% of the time
where the time goes in v5:
time: 93.4 us; the launch traced here: 93.3 us
  Pallas kernels  91.2 us (98%)
  local copies, waits for them, and re-layouts  2.06 us (2%)
    pallas_call x1, Pallas kernels, on_device(): pl.pallas_call(functools.partial(kernel, nz, nx), out_shape=jax.ShapeDtyp...  91.2 us
    unnamed x1, local copies, waits for them, and re-layouts  2.06 us

profile of v5, /device:TPU:33, one launch (start us, length us, event | category | flops | bytes accessed | tf_op | source)
XLA Modules:
  0.0 93.3 jit_solution(12240913038527961597)
XLA Ops:
  0.0 91.2 %mixing.1 = bf16[768,512]{1,0:T(8,128)(2,1)} custom-call(bf16[384,4096]{1,0:T(8,128)(2,1)} %latent.1, bf16[32,4096]{1,0:T(8,128)(2,1)} %context.1, bf16[256,512]{1,0:T(8,128)(2,1)} %shift_w.1, bf16[256,512]{1,0:T(8,128)(2,1)} %scale_w.1, bf16[256,512]{1,0:T(8,128)(2,1)} %gate_w.1, bf16[4096,256]{1,0:T(8,128)(2,1)} %og_w.1, bf16[4096,256]{1,0:T(8,128)(2,1)} %sg_w.1, ...), custom_call_target="tpu_custom_call" | custom-call | tf_op jit(solution)/shard_map/mixing/pallas_call | solution.py:1111
  91.2 2.1 %copy.23 = bf16[768,512]{1,0:T(8,128)(2,1)} copy(bf16[768,512]{1,0:T(8,128)(2,1)} %mixing.1) | data formatting | bytes 1572864
